TPU v7x, 32 devices: a whole 2x2x4 slice. The times are simulated.
32 devices in a mesh: fs: 8 (over z, y), tp: 4 (over x, core).
Axes of the slice: x: 2, y: 2, z: 4, core: 2. Of those that a mesh axis runs over, the one named last changes fastest.
Arguments:
- normed_input: bfloat16 [6144, 2048], P(('fs', 'tp')), may hold values from -6 to 6
- pre_act: bfloat16 [6144, 8192], P('fs', 'tp'), may hold values from -6 to 6
- out_grad: bfloat16 [6144, 2048], P(('fs', 'tp')), may hold values from -6 to 6
- up_weight: bfloat16 [2048, 8192], P('fs', 'tp'), may hold values from -0.125 to 0.125
- down_weight: bfloat16 [8192, 2048], P('tp', 'fs'), may hold values from -0.0625 to 0.0625
Outputs:
- input_grad: bfloat16 [6144, 2048], P(('fs', 'tp'))
- up_grad: float32 [2048, 8192], P('fs', 'tp')
- down_grad: float32 [8192, 2048], P('tp', 'fs')
All inputs are finite; a program needn't handle non-finite values.
Results may differ from a plain program's by a relative error of at most 0.014.
Values may be sent and summed in bfloat16 or wider, within the bound.
A program may use at most 128 MiB of HBM per device.

v0:
```python
import functools

import jax
import jax.numpy as jnp
from jax import lax
from jax.experimental import pallas as pl
from jax.experimental.pallas import tpu as pltpu
from jax.sharding import PartitionSpec as P

MESH = pl.DeviceIdType.MESH
BF16, F32 = jnp.bfloat16, jnp.float32
CHUNKS = 4
ACT_PARTS = 2
DN, UP = 0, 1
RIGHT, LEFT = 0, 1


def aligned(value, unit):
    return pl.multiple_of(value, unit)


class Dims:
    def __init__(self, fs, tp, tokens, d, hidden):
        self.fs, self.tp = fs, tp
        self.ny, self.nc = 2, 2
        self.nz, self.nx = fs // 2, tp // 2
        self.t, self.d, self.h = tokens, d, hidden
        self.rows = tokens * tp
        self.all_rows = self.rows * self.ny
        self.hh = hidden // self.ny
        self.df = d // fs
        self.dz = self.df * self.ny
        self.half = tokens // 2
        self.hc = self.hh // CHUNKS
        self.ha = self.hh // ACT_PARTS


def kernel(
    m, inp, act, og, upw, dnw, ig_out, ug_out, dg_out,
    og_all, in_all, acts, hid, dn_all, up_all,
    part_dn, part_up, slot_dn, slot_up, crecv, xr1, yr1, yr2, xr2,
    loc, ag_s, ag_r, wy_s, wy_r, tok_s, tok_r, act_s, act_r,
    rs_s, rs_r, fin_s, fin_r, fin_l, igc_s, igc_r, igx_s, igx_r,
):
    f, tt = lax.axis_index("fs"), lax.axis_index("tp")
    ny, nx, nz = m.ny, m.nx, m.nz
    z, y = f // ny, f % ny
    x, c = tt // 2, tt % 2
    yo, co = 1 - y, 1 - c
    sends = []

    def at(zz, yy, xx, cc):
        return (zz * ny + yy, xx * 2 + cc)

    y_dev, c_dev = at(z, yo, x, c), at(z, y, x, co)
    z_dev = (at(z + 1, y, x, c), at(z - 1, y, x, c))
    has_z = (z < nz - 1, z > 0)

    def x_at(k):
        return lax.rem(x + k, nx)

    def remote(src, dst, ss, rs, dev):
        return pltpu.make_async_remote_copy(
            src_ref=src, dst_ref=dst, send_sem=ss, recv_sem=rs,
            device_id=dev, device_id_type=MESH,
        )

    def go(copy, cond=None):
        if cond is None:
            copy.start()
        else:
            pl.when(cond)(copy.start)
        sends.append((cond, copy))

    def drain():
        for cond, copy in sends:
            if cond is None:
                copy.wait_send()
            else:
                pl.when(cond)(copy.wait_send)
        sends.clear()

    barrier = pltpu.get_barrier_semaphore()
    peers = [(None, y_dev), (None, c_dev)]
    peers += [(None, at(z, y, x_at(k), c)) for k in range(1, nx)]
    peers += [(has_z[RIGHT], z_dev[RIGHT]), (has_z[LEFT], z_dev[LEFT])]
    for cond, dev in peers:
        def hello(dev=dev):
            pl.semaphore_signal(barrier, inc=1, device_id=dev, device_id_type=MESH)
        hello() if cond is None else pl.when(cond)(hello)
    lines = jnp.where(z > 0, 1, 0) + jnp.where(z < nz - 1, 1, 0)
    pl.semaphore_wait(barrier, 1 + nx + lines)

    def slot(buf, yy, xx, cc):
        start = aligned(((yy * nx + xx) * 2 + cc) * m.t, m.t)
        return buf.at[pl.ds(start, m.t), :]

    def weight_view(w, ff):
        start = aligned(ff * m.df, m.df)
        if w == DN:
            return dn_all.at[:, pl.ds(start, m.df)]
        return up_all.at[pl.ds(start, m.df), :]

    def weight_own(w, yy):
        start = aligned(yy * m.hh, m.hh)
        if w == DN:
            return dnw.at[pl.ds(start, m.hh), :]
        return upw.at[:, pl.ds(start, m.hh)]

    def ag(w, u, side, k, receive=False):
        back = k + 1 if receive else k
        origin = jnp.clip(z - back if side == RIGHT else z + back, 0, nz - 1)
        view = weight_view(w, origin * ny + (y if u == 0 else yo))
        src = weight_own(w, y) if (u == 0 and k == 0) else view
        dev = z_dev[side]
        return remote(src, view, ag_s.at[w, u, side, k], ag_r.at[w, u, side, k], dev)

    def ag_sends(side, k):
        if side == RIGHT:
            return jnp.logical_and(z >= k, z < nz - 1)
        return jnp.logical_and(z <= nz - 1 - k, z > 0)

    def ag_step(w, u, k):
        for side in (RIGHT, LEFT):
            cond = ag_sends(side, k)
            if k > 0:
                pl.when(cond)(ag(w, u, side, k - 1, True).wait_recv)
            go(ag(w, u, side, k), cond)

    def ag_finish(w, u):
        for k in range(nz - 1):
            pl.when(jnp.logical_and(z == nz - 1, z >= k + 1))(
                ag(w, u, RIGHT, k, True).wait_recv)
            pl.when(jnp.logical_and(z == 0, z <= nz - 2 - k))(
                ag(w, u, LEFT, k, True).wait_recv)

    def weight_y(w, receive=False):
        ff = z * ny + (yo if receive else y)
        return remote(weight_own(w, yo), weight_view(w, ff), wy_s.at[w], wy_r.at[w], y_dev)

    class Rows:
        def __init__(self, a, src, buf):
            self.a, self.src, self.buf = a, src, buf

        def copy(self, index, src, where, dev):
            return remote(src, slot(self.buf, *where), tok_s.at[self.a, index],
                          tok_r.at[self.a, index], dev)

        def over_y(self, receive=False):
            return self.copy(0, self.src, (yo if receive else y, x, c), y_dev)

        def over_x(self, j, k, receive=False):
            yy = y if j == 0 else yo
            xx = x_at(nx - k) if receive else x
            src = self.src if j == 0 else slot(self.buf, yy, x, c)
            return self.copy(j * (nx - 1) + k, src, (yy, xx, c), at(z, y, x_at(k), c))

        def over_c(self, j, k, receive=False):
            yy = y if j == 0 else yo
            xx = x_at(nx - k) if k else x
            src = self.src if j == 0 and k == 0 else slot(self.buf, yy, xx, c)
            index = 1 + 2 * (nx - 1) + j * nx + k
            return self.copy(index, src, (yy, xx, co if receive else c), c_dev)

        def start_y(self):
            go(self.over_y())

        def start_x(self):
            for k in range(1, nx):
                go(self.over_x(0, k))
            go(self.over_c(0, 0))

        def relay_y(self):
            self.over_y(True).wait_recv()
            for k in range(1, nx):
                go(self.over_x(1, k))
            go(self.over_c(1, 0))

        def relay_x(self, j):
            for k in range(1, nx):
                self.over_x(j, k, True).wait_recv()
                go(self.over_c(j, k))

        def finish(self):
            for j in range(ny):
                for k in range(nx):
                    self.over_c(j, k, True).wait_recv()

    og_rows = Rows(0, og, og_all)
    in_rows = Rows(1, inp, in_all)

    def act_copy(part, receive=False):
        col = part * m.ha
        src = act.at[:, pl.ds(aligned(yo * m.hh + col, m.ha), m.ha)]
        row = aligned((yo if receive else y) * m.rows, m.rows)
        dst = acts.at[pl.ds(row, m.rows), pl.ds(col, m.ha)]
        return remote(src, dst, act_s.at[part], act_r.at[part], y_dev)

    local = [
        pltpu.make_async_copy(weight_own(DN, y), weight_view(DN, f), loc.at[0]),
        pltpu.make_async_copy(weight_own(UP, y), weight_view(UP, f), loc.at[1]),
        pltpu.make_async_copy(og, slot(og_all, y, x, c), loc.at[2]),
        pltpu.make_async_copy(inp, slot(in_all, y, x, c), loc.at[3]),
        pltpu.make_async_copy(
            act.at[:, pl.ds(aligned(y * m.hh, m.hh), m.hh)],
            acts.at[pl.ds(aligned(y * m.rows, m.rows), m.rows), :], loc.at[4]),
    ]

    parts, slots = (part_dn, part_up), (slot_dn, slot_up)

    def rs(w, side, target, ch, own):
        src = (parts if own else slots)[w].at[target, ch]
        if side == RIGHT:
            place = target
        else:
            place = jnp.where(target == z - 1, nz, target)
        return remote(src, slots[w].at[place, ch], rs_s.at[w, side, target, ch],
                      rs_r.at[w, side, target, ch], z_dev[side])

    def rs_waits(w, side, target, ch, place):
        return remote(parts[w].at[0, ch], slots[w].at[place, ch],
                      rs_s.at[w, side, target, ch], rs_r.at[w, side, target, ch],
                      z_dev[side])

    def by_rows(count, step, body):
        @pl.loop(0, count // step)
        def _(i):
            body(pl.ds(aligned(i * step, step), step))

    def rs_edge(w, target, ch):
        @pl.when(jnp.logical_and(z == 0, target > 0))
        def _():
            rs(w, RIGHT, target, ch, True).start()

        @pl.when(jnp.logical_and(z == nz - 1, target < nz - 1))
        def _():
            rs(w, LEFT, target, ch, True).start()

    def rs_relay(w, step):
        for side in (RIGHT, LEFT):
            target = nz - 1 - step if side == RIGHT else step
            if side == RIGHT:
                cond = jnp.logical_and(z > 0, z < target)
            else:
                cond = jnp.logical_and(z < nz - 1, z > target)

            @pl.when(cond)
            def _():
                @pl.loop(0, CHUNKS)
                def _(ch):
                    rs_waits(w, side, target, ch, target).wait_recv()
                    buf, own = slots[w].at[target, ch], parts[w].at[target, ch]

                    def add(rows):
                        buf[rows, :] = (buf[rows, :].astype(F32)
                                        + own[rows, :].astype(F32)).astype(BF16)
                    by_rows(buf.shape[0], 64, add)
                    rs(w, side, target, ch, False).start()

    def rs_drain(w):
        for target in range(nz):
            @pl.loop(0, CHUNKS)
            def _(ch):
                pl.when(z < target)(rs(w, RIGHT, target, ch, False).wait_send)
                pl.when(z > target)(rs(w, LEFT, target, ch, False).wait_send)

    def fin_copy(w, ch, yy, receive=False):
        src = parts[w].at[z, ch]
        if w == DN:
            src = src.at[:, pl.ds(aligned(yy * m.df, m.df), m.df)]
            row = aligned((yo if receive else y) * m.hh + ch * m.hc, m.hc)
            return src, dg_out.at[pl.ds(row, m.hc), :]
        src = src.at[pl.ds(aligned(yy * m.df, m.df), m.df), :]
        col = aligned((yo if receive else y) * m.hh + ch * m.hc, m.hc)
        return src, ug_out.at[:, pl.ds(col, m.hc)]

    def fin_remote(w, ch, receive=False):
        src, dst = fin_copy(w, ch, yo, receive)
        return remote(src, dst, fin_s.at[w, ch], fin_r.at[w, ch], y_dev)

    def fin_local(w, ch):
        src, dst = fin_copy(w, ch, y)
        return pltpu.make_async_copy(src, dst, fin_l.at[w, ch])

    def rs_finish(w):
        @pl.loop(0, CHUNKS)
        def _(ch):
            own = parts[w].at[z, ch]
            right, left = slots[w].at[z, ch], slots[w].at[nz, ch]
            pl.when(z > 0)(rs_waits(w, RIGHT, z, ch, z).wait_recv)
            pl.when(z < nz - 1)(rs_waits(w, LEFT, z, ch, nz).wait_recv)

            def total(*others):
                def add(rows):
                    value = own[rows, :].astype(F32)
                    for other in others:
                        value = value + other[rows, :].astype(F32)
                    own[rows, :] = value.astype(BF16)
                by_rows(own.shape[0], 64, add)

            pl.when(z == 0)(lambda: total(left))
            pl.when(z == nz - 1)(lambda: total(right))
            pl.when(jnp.logical_and(z > 0, z < nz - 1))(lambda: total(right, left))
            fin_remote(w, ch).start()
            fin_local(w, ch).start()

    def fin_wait(w):
        @pl.loop(0, CHUNKS)
        def _(ch):
            fin_remote(w, ch).wait_send()
            fin_remote(w, ch, True).wait_recv()
            fin_local(w, ch).wait()

    def targets(i):
        turn = i // 2
        return jnp.where(i % 2 == 0, nz - 1 - turn, turn)

    def squares():
        def body(rows):
            active = jnp.maximum(acts[rows, :].astype(F32), 0.0)
            hid[rows, :] = (active * active).astype(BF16)
        by_rows(m.all_rows, 64, body)

    def dot_rows(a, b):
        return lax.dot_general(a, b, (((0,), (0,)), ((), ())), preferred_element_type=F32)

    def dot_cols(a, b):
        return lax.dot_general(a, b, (((1,), (1,)), ((), ())), preferred_element_type=F32)

    def dot_dn():
        @pl.loop(0, nz * CHUNKS)
        def _(i):
            target, ch = targets(i // CHUNKS), i % CHUNKS
            a = hid[:, pl.ds(aligned(ch * m.hc, m.hc), m.hc)]
            b = og_all[:, pl.ds(aligned(target * m.dz, m.dz), m.dz)]
            part_dn[target, ch] = dot_rows(a, b).astype(BF16)
            rs_edge(DN, target, ch)

    def dot_hg():
        @pl.loop(0, m.all_rows // 256)
        def _(i):
            rows = pl.ds(aligned(i * 256, 256), 256)
            active = jnp.maximum(acts[rows, :].astype(F32), 0.0)
            grad = dot_cols(og_all[rows, :], dn_all[...])
            hid[rows, :] = (2.0 * active * grad).astype(BF16)

    def dot_up():
        @pl.loop(0, nz * CHUNKS)
        def _(i):
            target, ch = targets(i // CHUNKS), i % CHUNKS
            a = in_all[:, pl.ds(aligned(target * m.dz, m.dz), m.dz)]
            b = hid[:, pl.ds(aligned(ch * m.hc, m.hc), m.hc)]
            part_up[target, ch] = dot_rows(a, b).astype(BF16)
            rs_edge(UP, target, ch)

    part = og_all

    def ig_c(j, receive=False):
        yy, xx = j // nx, j % nx
        return remote(slot(part, yy, xx, co), crecv.at[yy, xx], igc_s.at[j], igc_r.at[j], c_dev)

    def dot_in():
        @pl.loop(0, 2 * ny * nx)
        def _(i):
            j = i % (ny * nx)
            cc = jnp.where(i < ny * nx, co, c)
            rows = pl.ds(aligned((j * 2 + cc) * m.t, m.t), m.t)
            part[rows, :] = dot_cols(hid[rows, :], up_all[...]).astype(BF16)
            pl.when(i < ny * nx)(ig_c(j).start)

    def ig_sum():
        @pl.loop(0, ny * nx)
        def _(j):
            ig_c(j).wait_recv()
            buf, own = crecv.at[j // nx, j % nx], slot(part, j // nx, j % nx, c)

            def add(rows):
                buf[rows, :] = (buf[rows, :].astype(F32) + own[rows, :].astype(F32)).astype(BF16)
            by_rows(m.t, 32, add)

    low, high = pl.ds(0, m.half), pl.ds(m.half, m.half)

    def accumulate(dst, others):
        def add(rows):
            value = dst[rows, :].astype(F32)
            for other in others:
                value = value + other[rows, :].astype(F32)
            dst[rows, :] = value.astype(BF16)
        by_rows(m.half, 32, add)

    def ig_x1(k):
        return remote(crecv.at[:, x_at(k), low, :], xr1.at[k - 1],
                      igx_s.at[0, k], igx_r.at[0, k], at(z, y, x_at(k), c))

    def ig_y1():
        return remote(crecv.at[yo, x, low, :], yr1, igx_s.at[1, 0], igx_r.at[1, 0], y_dev)

    def ig_y2():
        return remote(crecv.at[yo, :, high, :], yr2, igx_s.at[2, 0], igx_r.at[2, 0], y_dev)

    def ig_x2(k):
        return remote(crecv.at[y, x_at(k), high, :], xr2.at[k - 1],
                      igx_s.at[3, k], igx_r.at[3, k], at(z, y, x_at(k), c))

    def ig_first():
        for k in range(1, nx):
            go(ig_x1(k))
        go(ig_y2())

    def ig_second():
        for k in range(1, nx):
            ig_x1(k).wait_recv()
        for yy in range(ny):
            accumulate(crecv.at[yy, x, low, :], [xr1.at[k, yy] for k in range(nx - 1)])
        go(ig_y1())
        ig_y2().wait_recv()
        for xx in range(nx):
            accumulate(crecv.at[y, xx, high, :], [yr2.at[xx]])
        for k in range(1, nx):
            go(ig_x2(k))

    ig_local = pltpu.make_async_copy(crecv.at[y, x], ig_out, loc.at[5])

    def ig_last():
        ig_y1().wait_recv()
        accumulate(crecv.at[y, x, low, :], [yr1])
        for k in range(1, nx):
            ig_x2(k).wait_recv()
        accumulate(crecv.at[y, x, high, :], [xr2.at[k] for k in range(nx - 1)])
        ig_local.start()

    ag_step(DN, 0, 0)
    og_rows.start_y()
    og_rows.start_x()
    go(weight_y(DN))
    for part_index in range(ACT_PARTS):
        go(act_copy(part_index))
    for copy in local:
        copy.start()
    for copy in local:
        copy.wait()
    ag_step(DN, 0, 1)
    og_rows.relay_y()
    og_rows.relay_x(0)
    for k in range(2, nz - 1):
        ag_step(DN, 0, k)
    weight_y(DN, True).wait_recv()
    ag_step(DN, 1, 0)
    ag_step(UP, 0, 0)
    og_rows.relay_x(1)
    in_rows.start_y()
    in_rows.start_x()
    go(weight_y(UP))
    ag_step(DN, 1, 1)
    og_rows.finish()
    for part_index in range(ACT_PARTS):
        act_copy(part_index, True).wait_recv()
    for k in range(2, nz - 1):
        ag_step(DN, 1, k)
    squares()
    dot_dn()
    ag_step(UP, 0, 1)
    in_rows.relay_y()
    in_rows.relay_x(0)
    rs_relay(DN, 0)
    for k in range(2, nz - 1):
        ag_step(UP, 0, k)
    weight_y(UP, True).wait_recv()
    ag_step(UP, 1, 0)
    in_rows.relay_x(1)
    ag_finish(DN, 0)
    ag_finish(DN, 1)
    dot_hg()
    in_rows.finish()
    dot_up()
    ag_step(UP, 1, 1)
    for step in range(1, nz - 1):
        rs_relay(DN, step)
    for k in range(2, nz - 1):
        ag_step(UP, 1, k)
    rs_relay(UP, 0)
    rs_finish(DN)
    ag_finish(UP, 0)
    ag_finish(UP, 1)
    drain()
    dot_in()
    for step in range(1, nz - 1):
        rs_relay(UP, step)
    ig_sum()
    ig_first()
    ig_second()
    ig_last()
    rs_finish(UP)
    drain()

    @pl.loop(0, ny * nx)
    def _(j):
        ig_c(j).wait_send()

    rs_drain(DN)
    rs_drain(UP)
    ig_local.wait()
    fin_wait(DN)
    fin_wait(UP)


def local_step(fs, tp, inp, act, og, upw, dnw):
    m = Dims(fs, tp, og.shape[0], og.shape[1], act.shape[1])
    dma = pltpu.SemaphoreType.DMA
    vm = pltpu.VMEM
    any_space = pl.BlockSpec(memory_space=pl.ANY)
    rows_events = 1 + 2 * (m.nx - 1) + m.ny * m.nx
    flops = 8 * m.all_rows * m.hh * m.d
    ig, ug, dg = pl.pallas_call(
        functools.partial(kernel, m),
        name="ffn_backward",
        out_shape=(
            jax.ShapeDtypeStruct((m.t, m.d), BF16),
            jax.ShapeDtypeStruct((m.df, m.h), BF16),
            jax.ShapeDtypeStruct((m.h, m.df), BF16),
        ),
        in_specs=[any_space] * 5,
        out_specs=(any_space,) * 3,
        scratch_shapes=[
            vm((m.all_rows, m.d), BF16),
            vm((m.all_rows, m.d), BF16),
            vm((m.all_rows, m.hh), BF16),
            vm((m.all_rows, m.hh), BF16),
            vm((m.hh, m.d), BF16),
            vm((m.d, m.hh), BF16),
            vm((m.nz, CHUNKS, m.hc, m.dz), BF16),
            vm((m.nz, CHUNKS, m.dz, m.hc), BF16),
            vm((m.nz + 1, CHUNKS, m.hc, m.dz), BF16),
            vm((m.nz + 1, CHUNKS, m.dz, m.hc), BF16),
            vm((m.ny, m.nx, m.t, m.d), BF16),
            vm((m.nx - 1, m.ny, m.half, m.d), BF16),
            vm((m.half, m.d), BF16),
            vm((m.nx, m.half, m.d), BF16),
            vm((m.nx - 1, m.half, m.d), BF16),
            dma((6,)),
            dma((2, m.ny, 2, m.nz - 1)),
            dma((2, m.ny, 2, m.nz - 1)),
            dma((2,)),
            dma((2,)),
            dma((2, rows_events)),
            dma((2, rows_events)),
            dma((ACT_PARTS,)),
            dma((ACT_PARTS,)),
            dma((2, 2, m.nz, CHUNKS)),
            dma((2, 2, m.nz, CHUNKS)),
            dma((2, CHUNKS)),
            dma((2, CHUNKS)),
            dma((2, CHUNKS)),
            dma((m.ny * m.nx,)),
            dma((m.ny * m.nx,)),
            dma((4, m.nx)),
            dma((4, m.nx)),
        ],
        cost_estimate=pl.CostEstimate(flops=flops, bytes_accessed=2**25, transcendentals=0),
        compiler_params=pltpu.CompilerParams(
            collective_id=0, has_side_effects=True, vmem_limit_bytes=67043328
        ),
    )(inp, act, og, upw, dnw)
    return ig, ug.astype(F32), dg.astype(F32)


def solution(mesh):
    placed = (
        P(("fs", "tp"), None),
        P("fs", "tp"),
        P(("fs", "tp"), None),
        P("fs", "tp"),
        P("tp", "fs"),
    )
    return jax.shard_map(
        functools.partial(local_step, mesh.shape["fs"], mesh.shape["tp"]),
        mesh=mesh,
        in_specs=placed,
        out_specs=(P(("fs", "tp"), None), P("fs", "tp"), P("tp", "fs")),
        check_vma=False,
    )
```

profile of v0, /device:TPU:8, one launch (start us, length us, event | category | flops | bytes accessed | tf_op | source)
XLA Modules:
  0.0 293.0 jit_solution(7983571801523297748)
XLA Ops:
  0.6 287.1 %ffn_backward.1 = (bf16[192,2048]{1,0:T(8,128)(2,1)}, bf16[256,2048]{1,0:T(8,128)(2,1)}, bf16[2048,256]{1,0:T(8,128)(2,1)}) custom-call(bf16[192,2048]{1,0:T(8,128)(2,1)} %inp.1, bf16[768,2048]{1,0:T(8,128)(2,1)} %act.1, bf16[192,2048]{1,0:T(8,128)(2,1)} %og.1, bf16[256,2048]{1,0:T(8,128)(2,1)} %upw.1, bf16[2048,256]{1,0:T(8,128)(2,1)} %dnw.1), custom_call_target="tpu_custom_call" | custom-call | flops 25769803776 | bytes 33554432 | tf_op jit(solution)/shard_map/ffn_backward/pallas_call | solution.py:514
  287.7 0.0 copy-start
  287.7 2.9 convert_element_type.6
  290.6 0.0 copy-done
  290.6 0.0 copy-start.1
  290.6 1.5 convert_element_type.7
  292.1 0.0 copy-done.1
  292.1 0.9 copy.9
Async XLA Ops:
  287.7 2.9 copy-start
  290.6 1.5 copy-start.1
where the time goes:
time: 293 us
  Pallas kernels  287 us (98%)
  other arithmetic  4.36 us (1%)
    pallas_call x1, Pallas kernels, local_step(): pl.pallas_call(functools.partial(kernel, m), name='ffn_backward', out_sha...  287 us

commit v1 on v0

--- a/solution.py
+++ b/solution.py
@@ -10,7 +10,7 @@
 MESH = pl.DeviceIdType.MESH
 BF16, F32 = jnp.bfloat16, jnp.float32
 CHUNKS = 4
-ACT_PARTS = 2
+ACT_PARTS = 4
 DN, UP = 0, 1
 RIGHT, LEFT = 0, 1
 
@@ -65,20 +65,20 @@
             device_id=dev, device_id_type=MESH,
         )
 
-    def go(copy, cond=None):
+    def go(copy, cond=None, group=sends):
         if cond is None:
             copy.start()
         else:
             pl.when(cond)(copy.start)
-        sends.append((cond, copy))
-
-    def drain():
-        for cond, copy in sends:
+        group.append((cond, copy))
+
+    def drain(group):
+        for cond, copy in group:
             if cond is None:
                 copy.wait_send()
             else:
                 pl.when(cond)(copy.wait_send)
-        sends.clear()
+        group.clear()
 
     barrier = pltpu.get_barrier_semaphore()
     peers = [(None, y_dev), (None, c_dev)]
@@ -120,9 +120,15 @@
             return jnp.logical_and(z >= k, z < nz - 1)
         return jnp.logical_and(z <= nz - 1 - k, z > 0)
 
-    def ag_step(w, u, k):
+    def ag_step(w, u, k, where="all"):
+        outer = (z == 0, z == nz - 1)
+        inner = jnp.logical_and(z > 0, z < nz - 1)
         for side in (RIGHT, LEFT):
             cond = ag_sends(side, k)
+            if where == "edge":
+                cond = outer[side]
+            if where == "inner":
+                cond = inner
             if k > 0:
                 pl.when(cond)(ag(w, u, side, k - 1, True).wait_recv)
             go(ag(w, u, side, k), cond)
@@ -140,7 +146,13 @@
 
     class Rows:
         def __init__(self, a, src, buf):
-            self.a, self.src, self.buf = a, src, buf
+            self.a, self.src, self.buf, self.sends = a, src, buf, []
+
+        def go(self, copy):
+            go(copy, None, self.sends)
+
+        def drain(self):
+            drain(self.sends)
 
         def copy(self, index, src, where, dev):
             return remote(src, slot(self.buf, *where), tok_s.at[self.a, index],
@@ -163,23 +175,23 @@
             return self.copy(index, src, (yy, xx, co if receive else c), c_dev)
 
         def start_y(self):
-            go(self.over_y())
+            self.go(self.over_y())
 
         def start_x(self):
             for k in range(1, nx):
-                go(self.over_x(0, k))
-            go(self.over_c(0, 0))
+                self.go(self.over_x(0, k))
+            self.go(self.over_c(0, 0))
 
         def relay_y(self):
             self.over_y(True).wait_recv()
             for k in range(1, nx):
-                go(self.over_x(1, k))
-            go(self.over_c(1, 0))
+                self.go(self.over_x(1, k))
+            self.go(self.over_c(1, 0))
 
         def relay_x(self, j):
             for k in range(1, nx):
                 self.over_x(j, k, True).wait_recv()
-                go(self.over_c(j, k))
+                self.go(self.over_c(j, k))
 
         def finish(self):
             for j in range(ny):
@@ -236,26 +248,45 @@
         def _():
             rs(w, LEFT, target, ch, True).start()
 
-    def rs_relay(w, step):
-        for side in (RIGHT, LEFT):
-            target = nz - 1 - step if side == RIGHT else step
-            if side == RIGHT:
-                cond = jnp.logical_and(z > 0, z < target)
-            else:
-                cond = jnp.logical_and(z < nz - 1, z > target)
-
-            @pl.when(cond)
-            def _():
-                @pl.loop(0, CHUNKS)
-                def _(ch):
-                    rs_waits(w, side, target, ch, target).wait_recv()
-                    buf, own = slots[w].at[target, ch], parts[w].at[target, ch]
-
-                    def add(rows):
-                        buf[rows, :] = (buf[rows, :].astype(F32)
-                                        + own[rows, :].astype(F32)).astype(BF16)
-                    by_rows(buf.shape[0], 64, add)
-                    rs(w, side, target, ch, False).start()
+    def rs_pass(w, side, step, ch):
+        target = nz - 1 - step if side == RIGHT else step
+        if side == RIGHT:
+            cond = jnp.logical_and(z > 0, z < target)
+        else:
+            cond = jnp.logical_and(z < nz - 1, z > target)
+
+        @pl.when(cond)
+        def _():
+            rs_waits(w, side, target, ch, target).wait_recv()
+            buf, own = slots[w].at[target, ch], parts[w].at[target, ch]
+
+            def add(rows):
+                buf[rows, :] = (buf[rows, :].astype(F32)
+                                + own[rows, :].astype(F32)).astype(BF16)
+            by_rows(buf.shape[0], 64, add)
+            rs(w, side, target, ch, False).start()
+
+    def near(w, ch):
+        @pl.when(z < nz // 2)
+        def _():
+            for step in range(nz - 2):
+                rs_pass(w, RIGHT, step, ch)
+
+        @pl.when(z >= nz // 2)
+        def _():
+            for step in range(nz - 2):
+                rs_pass(w, LEFT, step, ch)
+
+    def far(w, ch):
+        @pl.when(z < nz // 2)
+        def _():
+            for step in range(nz - 2):
+                rs_pass(w, LEFT, step, ch)
+
+        @pl.when(z >= nz // 2)
+        def _():
+            for step in range(nz - 2):
+                rs_pass(w, RIGHT, step, ch)
 
     def rs_drain(w):
         for target in range(nz):
@@ -282,27 +313,25 @@
         src, dst = fin_copy(w, ch, y)
         return pltpu.make_async_copy(src, dst, fin_l.at[w, ch])
 
-    def rs_finish(w):
-        @pl.loop(0, CHUNKS)
-        def _(ch):
-            own = parts[w].at[z, ch]
-            right, left = slots[w].at[z, ch], slots[w].at[nz, ch]
-            pl.when(z > 0)(rs_waits(w, RIGHT, z, ch, z).wait_recv)
-            pl.when(z < nz - 1)(rs_waits(w, LEFT, z, ch, nz).wait_recv)
-
-            def total(*others):
-                def add(rows):
-                    value = own[rows, :].astype(F32)
-                    for other in others:
-                        value = value + other[rows, :].astype(F32)
-                    own[rows, :] = value.astype(BF16)
-                by_rows(own.shape[0], 64, add)
-
-            pl.when(z == 0)(lambda: total(left))
-            pl.when(z == nz - 1)(lambda: total(right))
-            pl.when(jnp.logical_and(z > 0, z < nz - 1))(lambda: total(right, left))
-            fin_remote(w, ch).start()
-            fin_local(w, ch).start()
+    def rs_finish(w, ch):
+        own = parts[w].at[z, ch]
+        right, left = slots[w].at[z, ch], slots[w].at[nz, ch]
+        pl.when(z > 0)(rs_waits(w, RIGHT, z, ch, z).wait_recv)
+        pl.when(z < nz - 1)(rs_waits(w, LEFT, z, ch, nz).wait_recv)
+
+        def total(*others):
+            def add(rows):
+                value = own[rows, :].astype(F32)
+                for other in others:
+                    value = value + other[rows, :].astype(F32)
+                own[rows, :] = value.astype(BF16)
+            by_rows(own.shape[0], 64, add)
+
+        pl.when(z == 0)(lambda: total(left))
+        pl.when(z == nz - 1)(lambda: total(right))
+        pl.when(jnp.logical_and(z > 0, z < nz - 1))(lambda: total(right, left))
+        fin_remote(w, ch).start()
+        fin_local(w, ch).start()
 
     def fin_wait(w):
         @pl.loop(0, CHUNKS)
@@ -315,10 +344,12 @@
         turn = i // 2
         return jnp.where(i % 2 == 0, nz - 1 - turn, turn)
 
-    def squares():
+    def squares(ch):
+        cols = pl.ds(ch * m.hc, m.hc)
+
         def body(rows):
-            active = jnp.maximum(acts[rows, :].astype(F32), 0.0)
-            hid[rows, :] = (active * active).astype(BF16)
+            active = jnp.maximum(acts[rows, cols].astype(F32), 0.0)
+            hid[rows, cols] = (active * active).astype(BF16)
         by_rows(m.all_rows, 64, body)
 
     def dot_rows(a, b):
@@ -327,11 +358,11 @@
     def dot_cols(a, b):
         return lax.dot_general(a, b, (((1,), (1,)), ((), ())), preferred_element_type=F32)
 
-    def dot_dn():
-        @pl.loop(0, nz * CHUNKS)
+    def dot_dn(ch):
+        @pl.loop(0, nz)
         def _(i):
-            target, ch = targets(i // CHUNKS), i % CHUNKS
-            a = hid[:, pl.ds(aligned(ch * m.hc, m.hc), m.hc)]
+            target = targets(i)
+            a = hid[:, pl.ds(ch * m.hc, m.hc)]
             b = og_all[:, pl.ds(aligned(target * m.dz, m.dz), m.dz)]
             part_dn[target, ch] = dot_rows(a, b).astype(BF16)
             rs_edge(DN, target, ch)
@@ -344,12 +375,12 @@
             grad = dot_cols(og_all[rows, :], dn_all[...])
             hid[rows, :] = (2.0 * active * grad).astype(BF16)
 
-    def dot_up():
-        @pl.loop(0, nz * CHUNKS)
+    def dot_up(ch):
+        @pl.loop(0, nz)
         def _(i):
-            target, ch = targets(i // CHUNKS), i % CHUNKS
+            target = targets(i)
             a = in_all[:, pl.ds(aligned(target * m.dz, m.dz), m.dz)]
-            b = hid[:, pl.ds(aligned(ch * m.hc, m.hc), m.hc)]
+            b = hid[:, pl.ds(ch * m.hc, m.hc)]
             part_up[target, ch] = dot_rows(a, b).astype(BF16)
             rs_edge(UP, target, ch)
 
@@ -359,14 +390,14 @@
         yy, xx = j // nx, j % nx
         return remote(slot(part, yy, xx, co), crecv.at[yy, xx], igc_s.at[j], igc_r.at[j], c_dev)
 
-    def dot_in():
-        @pl.loop(0, 2 * ny * nx)
-        def _(i):
-            j = i % (ny * nx)
-            cc = jnp.where(i < ny * nx, co, c)
+    def dot_in(remote_half):
+        @pl.loop(0, ny * nx)
+        def _(j):
+            cc = co if remote_half else c
             rows = pl.ds(aligned((j * 2 + cc) * m.t, m.t), m.t)
             part[rows, :] = dot_cols(hid[rows, :], up_all[...]).astype(BF16)
-            pl.when(i < ny * nx)(ig_c(j).start)
+            if remote_half:
+                ig_c(j).start()
 
     def ig_sum():
         @pl.loop(0, ny * nx)
@@ -429,79 +460,130 @@
         accumulate(crecv.at[y, x, high, :], [xr2.at[k] for k in range(nx - 1)])
         ig_local.start()
 
-    ag_step(DN, 0, 0)
-    og_rows.start_y()
-    og_rows.start_x()
-    go(weight_y(DN))
-    for part_index in range(ACT_PARTS):
-        go(act_copy(part_index))
-    for copy in local:
-        copy.start()
-    for copy in local:
-        copy.wait()
-    ag_step(DN, 0, 1)
-    og_rows.relay_y()
-    og_rows.relay_x(0)
-    for k in range(2, nz - 1):
-        ag_step(DN, 0, k)
-    weight_y(DN, True).wait_recv()
-    ag_step(DN, 1, 0)
-    ag_step(UP, 0, 0)
-    og_rows.relay_x(1)
-    in_rows.start_y()
-    in_rows.start_x()
-    go(weight_y(UP))
-    ag_step(DN, 1, 1)
-    og_rows.finish()
-    for part_index in range(ACT_PARTS):
-        act_copy(part_index, True).wait_recv()
-    for k in range(2, nz - 1):
-        ag_step(DN, 1, k)
-    squares()
-    dot_dn()
-    ag_step(UP, 0, 1)
-    in_rows.relay_y()
-    in_rows.relay_x(0)
-    rs_relay(DN, 0)
-    for k in range(2, nz - 1):
-        ag_step(UP, 0, k)
-    weight_y(UP, True).wait_recv()
-    ag_step(UP, 1, 0)
-    in_rows.relay_x(1)
-    ag_finish(DN, 0)
-    ag_finish(DN, 1)
-    dot_hg()
-    in_rows.finish()
-    dot_up()
-    ag_step(UP, 1, 1)
-    for step in range(1, nz - 1):
-        rs_relay(DN, step)
-    for k in range(2, nz - 1):
-        ag_step(UP, 1, k)
-    rs_relay(UP, 0)
-    rs_finish(DN)
-    ag_finish(UP, 0)
-    ag_finish(UP, 1)
-    drain()
-    dot_in()
-    for step in range(1, nz - 1):
-        rs_relay(UP, step)
-    ig_sum()
-    ig_first()
-    ig_second()
-    ig_last()
-    rs_finish(UP)
-    drain()
-
-    @pl.loop(0, ny * nx)
-    def _(j):
-        ig_c(j).wait_send()
-
-    rs_drain(DN)
-    rs_drain(UP)
-    ig_local.wait()
-    fin_wait(DN)
-    fin_wait(UP)
+    def acts_in(index):
+        act_copy(index, True).wait_recv()
+
+    def start():
+        ag_step(DN, 0, 0)
+        og_rows.start_y()
+        og_rows.start_x()
+        go(weight_y(DN))
+        go(act_copy(0))
+        go(act_copy(1))
+        go(weight_y(UP))
+        go(act_copy(2))
+        go(act_copy(3))
+        in_rows.start_y()
+        ag_step(UP, 0, 0, "edge")
+        for copy in local:
+            copy.start()
+
+    def local_wait():
+        for copy in local:
+            copy.wait()
+
+    def weight_in(w):
+        weight_y(w, True).wait_recv()
+
+    def ig_drain():
+        @pl.loop(0, ny * nx)
+        def _(j):
+            ig_c(j).wait_send()
+        ig_local.wait()
+
+    def steps(function, *args, first=2):
+        return [(function, *args, k) for k in range(first, nz - 1)]
+
+    plan = [
+        (start,),
+        (ag_step, DN, 0, 1),
+        (og_rows.relay_y,),
+        (og_rows.relay_x, 0),
+        (in_rows.start_x,),
+        *steps(ag_step, DN, 0),
+        (weight_in, DN),
+        (ag_step, DN, 1, 0),
+        (og_rows.relay_x, 1),
+        (og_rows.finish,),
+        (local_wait,),
+        (acts_in, 0),
+        (squares, 0),
+        (dot_dn, 0),
+        (ag_step, DN, 1, 1),
+        (acts_in, 1),
+        (squares, 1),
+        (dot_dn, 1),
+        (near, DN, 0),
+        *steps(ag_step, DN, 1),
+        (ag_step, UP, 0, 0, "inner"),
+        (weight_in, UP),
+        (far, DN, 0),
+        (acts_in, 2),
+        (squares, 2),
+        (dot_dn, 2),
+        (near, DN, 1),
+        (ag_step, UP, 0, 1),
+        (acts_in, 3),
+        (squares, 3),
+        (dot_dn, 3),
+        (ag_finish, DN, 0),
+        (ag_finish, DN, 1),
+        (dot_hg,),
+        (near, DN, 2),
+        (far, DN, 1),
+        *steps(ag_step, UP, 0),
+        (ag_step, UP, 1, 0),
+        (in_rows.relay_y,),
+        (in_rows.relay_x, 0),
+        (near, DN, 3),
+        (far, DN, 2),
+        (ag_step, UP, 1, 1),
+        (in_rows.relay_x, 1),
+        (in_rows.finish,),
+        (dot_up, 0),
+        (far, DN, 3),
+        *steps(ag_step, UP, 1),
+        (dot_up, 1),
+        (dot_up, 2),
+        (dot_up, 3),
+        (near, UP, 0),
+        (rs_finish, DN, 0),
+        (rs_finish, DN, 1),
+        (far, UP, 0),
+        (near, UP, 1),
+        (rs_finish, DN, 2),
+        (rs_finish, DN, 3),
+        (ag_finish, UP, 0),
+        (ag_finish, UP, 1),
+        (og_rows.drain,),
+        (dot_in, True),
+        (far, UP, 1),
+        (near, UP, 2),
+        (dot_in, False),
+        (ig_sum,),
+        (ig_first,),
+        (rs_finish, UP, 0),
+        (far, UP, 2),
+        (near, UP, 3),
+        (rs_finish, UP, 1),
+        (far, UP, 3),
+        (ig_second,),
+        (rs_finish, UP, 2),
+        (ig_last,),
+        (rs_finish, UP, 3),
+        (in_rows.drain,),
+        (drain, sends),
+        (ig_drain,),
+        (rs_drain, DN),
+        (rs_drain, UP),
+        (fin_wait, DN),
+        (fin_wait, UP),
+    ]
+    for index, (function, *args) in enumerate(plan):
+        tags = [str(arg) for arg in args if not isinstance(arg, list)]
+        label = "_".join([str(index), function.__name__, *tags])
+        with jax.named_scope(label):
+            function(*args)
 
 
 def local_step(fs, tp, inp, act, og, upw, dnw):

time: 293 us -> 229 us (0.78); the launches traced: 293 us -> 226 us
  Pallas kernels: 287 us -> 220 us
    pallas_call x1, Pallas kernels: 287 us -> 220 us  [local_step(): pl.pallas_call(functools.partial(kernel, m), name='ffn_backward', out_sha...]
where the time goes in v1:
time: 229 us; the launch traced here: 226 us
  Pallas kernels  220 us (96%)
  other arithmetic  4.36 us (2%)
    pallas_call x1, Pallas kernels, local_step(): pl.pallas_call(functools.partial(kernel, m), name='ffn_backward', out_sha...  220 us

profile of v1, /device:TPU:8, one launch (start us, length us, event | category | flops | bytes accessed | tf_op | source)
XLA Modules:
  0.0 225.8 jit_solution(17250897605475591995)
XLA Ops:
  0.6 219.9 %ffn_backward.1 = (bf16[192,2048]{1,0:T(8,128)(2,1)}, bf16[256,2048]{1,0:T(8,128)(2,1)}, bf16[2048,256]{1,0:T(8,128)(2,1)}) custom-call(bf16[192,2048]{1,0:T(8,128)(2,1)} %inp.1, bf16[768,2048]{1,0:T(8,128)(2,1)} %act.1, bf16[192,2048]{1,0:T(8,128)(2,1)} %og.1, bf16[256,2048]{1,0:T(8,128)(2,1)} %upw.1, bf16[2048,256]{1,0:T(8,128)(2,1)} %dnw.1), custom_call_target="tpu_custom_call" | custom-call | flops 25769803776 | bytes 33554432 | tf_op jit(solution)/shard_map/ffn_backward/pallas_call | solution.py:596
  220.5 0.0 copy-start
  220.5 2.9 %convert_element_type.6 = f32[256,2048]{1,0:T(8,128)} convert(bf16[256,2048]{1,0:T(8,128)(2,1)} %get-tuple-element.7) | non-fusion elementwise | flops 524288 | bytes 3145728 | tf_op jit(solution)/shard_map/convert_element_type | solution.py:646
  223.4 0.0 copy-done
  223.4 0.0 copy-start.1
  223.4 1.5 convert_element_type.7
  224.9 0.0 copy-done.1
  224.9 0.9 copy.9
Async XLA Ops:
  220.5 2.9 %copy-start = (bf16[2048,256]{1,0:T(8,128)(2,1)S(1)}, bf16[2048,256]{1,0:T(8,128)(2,1)}, u32[]{:S(2)}) copy-start(bf16[2048,256]{1,0:T(8,128)(2,1)} %get-tuple-element.8) | copy-start | bytes 3145732
  223.4 1.5 copy-start.1

commit v2 on v1

--- a/solution.py
+++ b/solution.py
@@ -37,7 +37,7 @@
 
 def kernel(
     m, inp, act, og, upw, dnw, ig_out, ug_out, dg_out,
-    og_all, in_all, acts, hid, dn_all, up_all,
+    og_all, in_all, acts, hid, pre, dn_all, up_all,
     part_dn, part_up, slot_dn, slot_up, crecv, xr1, yr1, yr2, xr2,
     loc, ag_s, ag_r, wy_s, wy_r, tok_s, tok_r, act_s, act_r,
     rs_s, rs_r, fin_s, fin_r, fin_l, igc_s, igc_r, igx_s, igx_r,
@@ -95,58 +95,73 @@
         start = aligned(((yy * nx + xx) * 2 + cc) * m.t, m.t)
         return buf.at[pl.ds(start, m.t), :]
 
-    def weight_view(w, ff):
-        start = aligned(ff * m.df, m.df)
+    parts_of = (1, 2)
+
+    def weight_view(w, ff, h=None):
+        start, size = ff * m.df, m.df
         if w == DN:
-            return dn_all.at[:, pl.ds(start, m.df)]
-        return up_all.at[pl.ds(start, m.df), :]
-
-    def weight_own(w, yy):
+            return dn_all.at[:, pl.ds(aligned(start, m.df), m.df)]
+        if h is not None:
+            size = m.df // parts_of[w]
+            start = start + h * size
+        return up_all.at[pl.ds(aligned(start, size), size), :]
+
+    def weight_own(w, yy, h=None):
         start = aligned(yy * m.hh, m.hh)
         if w == DN:
             return dnw.at[pl.ds(start, m.hh), :]
-        return upw.at[:, pl.ds(start, m.hh)]
-
-    def ag(w, u, side, k, receive=False):
+        first, size = 0, m.df
+        if h is not None:
+            size = m.df // parts_of[w]
+            first = h * size
+        return upw.at[pl.ds(first, size), pl.ds(start, m.hh)]
+
+    def ag(w, u, h, side, k, receive=False):
         back = k + 1 if receive else k
         origin = jnp.clip(z - back if side == RIGHT else z + back, 0, nz - 1)
-        view = weight_view(w, origin * ny + (y if u == 0 else yo))
-        src = weight_own(w, y) if (u == 0 and k == 0) else view
-        dev = z_dev[side]
-        return remote(src, view, ag_s.at[w, u, side, k], ag_r.at[w, u, side, k], dev)
+        view = weight_view(w, origin * ny + (y if u == 0 else yo), h)
+        src = weight_own(w, y, h) if (u == 0 and k == 0) else view
+        return remote(src, view, ag_s.at[w, u, h, side, k], ag_r.at[w, u, h, side, k],
+                      z_dev[side])
 
     def ag_sends(side, k):
         if side == RIGHT:
             return jnp.logical_and(z >= k, z < nz - 1)
         return jnp.logical_and(z <= nz - 1 - k, z > 0)
 
-    def ag_step(w, u, k, where="all"):
+    def ag_step(w, u, h, k, where="all"):
         outer = (z == 0, z == nz - 1)
         inner = jnp.logical_and(z > 0, z < nz - 1)
+        close = (z < nz // 2, z >= nz // 2)
         for side in (RIGHT, LEFT):
             cond = ag_sends(side, k)
             if where == "edge":
                 cond = outer[side]
             if where == "inner":
                 cond = inner
+            if where == "near":
+                cond = jnp.logical_and(cond, close[side])
+            if where == "far":
+                cond = jnp.logical_and(cond, close[1 - side])
             if k > 0:
-                pl.when(cond)(ag(w, u, side, k - 1, True).wait_recv)
-            go(ag(w, u, side, k), cond)
-
-    def ag_finish(w, u):
+                pl.when(cond)(ag(w, u, h, side, k - 1, True).wait_recv)
+            go(ag(w, u, h, side, k), cond)
+
+    def ag_finish(w, u, h):
         for k in range(nz - 1):
             pl.when(jnp.logical_and(z == nz - 1, z >= k + 1))(
-                ag(w, u, RIGHT, k, True).wait_recv)
+                ag(w, u, h, RIGHT, k, True).wait_recv)
             pl.when(jnp.logical_and(z == 0, z <= nz - 2 - k))(
-                ag(w, u, LEFT, k, True).wait_recv)
+                ag(w, u, h, LEFT, k, True).wait_recv)
 
     def weight_y(w, receive=False):
         ff = z * ny + (yo if receive else y)
         return remote(weight_own(w, yo), weight_view(w, ff), wy_s.at[w], wy_r.at[w], y_dev)
 
     class Rows:
-        def __init__(self, a, src, buf):
-            self.a, self.src, self.buf, self.sends = a, src, buf, []
+        def __init__(self, a, src, buf, pieces):
+            self.a, self.buf, self.sends = a, buf, []
+            self.pieces, self.width, self.source = pieces, m.d // pieces, src
 
         def go(self, copy):
             go(copy, None, self.sends)
@@ -154,52 +169,61 @@
         def drain(self):
             drain(self.sends)
 
-        def copy(self, index, src, where, dev):
-            return remote(src, slot(self.buf, *where), tok_s.at[self.a, index],
+        def src(self, p):
+            return self.source.at[:, pl.ds(p * self.width, self.width)]
+
+        def place(self, p, yy, xx, cc):
+            start = aligned(((yy * nx + xx) * 2 + cc) * m.t, m.t)
+            return self.buf.at[pl.ds(start, m.t), pl.ds(p * self.width, self.width)]
+
+        def copy(self, p, index, src, where, dev):
+            index = index * self.pieces + p
+            return remote(src, self.place(p, *where), tok_s.at[self.a, index],
                           tok_r.at[self.a, index], dev)
 
-        def over_y(self, receive=False):
-            return self.copy(0, self.src, (yo if receive else y, x, c), y_dev)
-
-        def over_x(self, j, k, receive=False):
+        def over_y(self, p, receive=False):
+            return self.copy(p, 0, self.src(p), (yo if receive else y, x, c), y_dev)
+
+        def over_x(self, p, j, k, receive=False):
             yy = y if j == 0 else yo
             xx = x_at(nx - k) if receive else x
-            src = self.src if j == 0 else slot(self.buf, yy, x, c)
-            return self.copy(j * (nx - 1) + k, src, (yy, xx, c), at(z, y, x_at(k), c))
-
-        def over_c(self, j, k, receive=False):
+            src = self.src(p) if j == 0 else self.place(p, yy, x, c)
+            index = 1 + j * (nx - 1) + k - 1
+            return self.copy(p, index, src, (yy, xx, c), at(z, y, x_at(k), c))
+
+        def over_c(self, p, j, k, receive=False):
             yy = y if j == 0 else yo
             xx = x_at(nx - k) if k else x
-            src = self.src if j == 0 and k == 0 else slot(self.buf, yy, xx, c)
+            src = self.src(p) if j == 0 and k == 0 else self.place(p, yy, xx, c)
             index = 1 + 2 * (nx - 1) + j * nx + k
-            return self.copy(index, src, (yy, xx, co if receive else c), c_dev)
-
-        def start_y(self):
-            self.go(self.over_y())
-
-        def start_x(self):
+            return self.copy(p, index, src, (yy, xx, co if receive else c), c_dev)
+
+        def start_y(self, p):
+            self.go(self.over_y(p))
+
+        def start_x(self, p):
             for k in range(1, nx):
-                self.go(self.over_x(0, k))
-            self.go(self.over_c(0, 0))
-
-        def relay_y(self):
-            self.over_y(True).wait_recv()
+                self.go(self.over_x(p, 0, k))
+            self.go(self.over_c(p, 0, 0))
+
+        def relay_y(self, p):
+            self.over_y(p, True).wait_recv()
             for k in range(1, nx):
-                self.go(self.over_x(1, k))
-            self.go(self.over_c(1, 0))
-
-        def relay_x(self, j):
+                self.go(self.over_x(p, 1, k))
+            self.go(self.over_c(p, 1, 0))
+
+        def relay_x(self, p, j):
             for k in range(1, nx):
-                self.over_x(j, k, True).wait_recv()
-                self.go(self.over_c(j, k))
-
-        def finish(self):
+                self.over_x(p, j, k, True).wait_recv()
+                self.go(self.over_c(p, j, k))
+
+        def finish(self, p):
             for j in range(ny):
                 for k in range(nx):
-                    self.over_c(j, k, True).wait_recv()
-
-    og_rows = Rows(0, og, og_all)
-    in_rows = Rows(1, inp, in_all)
+                    self.over_c(p, j, k, True).wait_recv()
+
+    og_rows = Rows(0, og, og_all, nz)
+    in_rows = Rows(1, inp, in_all, 1)
 
     def act_copy(part, receive=False):
         col = part * m.ha
@@ -266,15 +290,15 @@
             by_rows(buf.shape[0], 64, add)
             rs(w, side, target, ch, False).start()
 
-    def near(w, ch):
+    def near(w, ch, first=0, last=nz - 2):
         @pl.when(z < nz // 2)
         def _():
-            for step in range(nz - 2):
+            for step in range(first, last):
                 rs_pass(w, RIGHT, step, ch)
 
         @pl.when(z >= nz // 2)
         def _():
-            for step in range(nz - 2):
+            for step in range(first, last):
                 rs_pass(w, LEFT, step, ch)
 
     def far(w, ch):
@@ -344,6 +368,8 @@
         turn = i // 2
         return jnp.where(i % 2 == 0, nz - 1 - turn, turn)
 
+    order = [nz - 1 - i // 2 if i % 2 == 0 else i // 2 for i in range(nz)]
+
     def squares(ch):
         cols = pl.ds(ch * m.hc, m.hc)
 
@@ -358,8 +384,8 @@
     def dot_cols(a, b):
         return lax.dot_general(a, b, (((1,), (1,)), ((), ())), preferred_element_type=F32)
 
-    def dot_dn(ch):
-        @pl.loop(0, nz)
+    def dot_dn(ch, first=0, last=nz):
+        @pl.loop(first, last)
         def _(i):
             target = targets(i)
             a = hid[:, pl.ds(ch * m.hc, m.hc)]
@@ -367,43 +393,66 @@
             part_dn[target, ch] = dot_rows(a, b).astype(BF16)
             rs_edge(DN, target, ch)
 
-    def dot_hg():
-        @pl.loop(0, m.all_rows // 256)
+    def dot_hg(ch):
+        cols = pl.ds(ch * m.hc, m.hc)
+
+        @pl.loop(0, m.all_rows // 512)
         def _(i):
-            rows = pl.ds(aligned(i * 256, 256), 256)
-            active = jnp.maximum(acts[rows, :].astype(F32), 0.0)
-            grad = dot_cols(og_all[rows, :], dn_all[...])
-            hid[rows, :] = (2.0 * active * grad).astype(BF16)
+            rows = pl.ds(aligned(i * 512, 512), 512)
+            active = jnp.maximum(acts[rows, cols].astype(F32), 0.0)
+            grad = dot_cols(og_all[rows, :], dn_all[cols, :])
+            pre[rows, cols] = (2.0 * active * grad).astype(BF16)
 
     def dot_up(ch):
         @pl.loop(0, nz)
         def _(i):
             target = targets(i)
             a = in_all[:, pl.ds(aligned(target * m.dz, m.dz), m.dz)]
-            b = hid[:, pl.ds(ch * m.hc, m.hc)]
+            b = pre[:, pl.ds(ch * m.hc, m.hc)]
             part_up[target, ch] = dot_rows(a, b).astype(BF16)
             rs_edge(UP, target, ch)
 
     part = og_all
-
-    def ig_c(j, receive=False):
+    width = m.d // 2
+    sets = [pl.ds(0, width), pl.ds(width, width)]
+
+    def ig_c(g, j):
         yy, xx = j // nx, j % nx
-        return remote(slot(part, yy, xx, co), crecv.at[yy, xx], igc_s.at[j], igc_r.at[j], c_dev)
-
-    def dot_in(remote_half):
+        return remote(slot(part, yy, xx, co).at[:, sets[g]], crecv.at[yy, xx, :, sets[g]],
+                      igc_s.at[g, j], igc_r.at[g, j], c_dev)
+
+    def dot_in(g, remote_half):
+        piece = m.df // 2
+        group = 4
+        tile = piece * group
+        cc = co if remote_half else c
+        count = m.fs // group
+
+        @pl.loop(0, ny * count)
+        def _(i):
+            yy, n = i // count, i % count
+            cols = pl.ds(aligned(g * width + n * tile, tile), tile)
+            blocks = [pl.ds(aligned(((yy * nx + xx) * 2 + cc) * m.t, m.t), m.t)
+                      for xx in range(nx)]
+            rows_of = [pl.ds(aligned((n * group + q) * m.df + g * piece, piece), piece)
+                       for q in range(group)]
+            a = jnp.concatenate([pre[rows, :] for rows in blocks], 0)
+            b = jnp.concatenate([up_all[rows, :] for rows in rows_of], 0)
+            value = dot_cols(a, b).astype(BF16)
+            for xx, rows in enumerate(blocks):
+                part[rows, cols] = value[xx * m.t:(xx + 1) * m.t]
+            if remote_half:
+                @pl.when(n == count - 1)
+                def _():
+                    for xx in range(nx):
+                        ig_c(g, yy * nx + xx).start()
+
+    def ig_sum(g):
         @pl.loop(0, ny * nx)
         def _(j):
-            cc = co if remote_half else c
-            rows = pl.ds(aligned((j * 2 + cc) * m.t, m.t), m.t)
-            part[rows, :] = dot_cols(hid[rows, :], up_all[...]).astype(BF16)
-            if remote_half:
-                ig_c(j).start()
-
-    def ig_sum():
-        @pl.loop(0, ny * nx)
-        def _(j):
-            ig_c(j).wait_recv()
-            buf, own = crecv.at[j // nx, j % nx], slot(part, j // nx, j % nx, c)
+            ig_c(g, j).wait_recv()
+            buf = crecv.at[j // nx, j % nx, :, sets[g]]
+            own = slot(part, j // nx, j % nx, c).at[:, sets[g]]
 
             def add(rows):
                 buf[rows, :] = (buf[rows, :].astype(F32) + own[rows, :].astype(F32)).astype(BF16)
@@ -419,64 +468,96 @@
             dst[rows, :] = value.astype(BF16)
         by_rows(m.half, 32, add)
 
-    def ig_x1(k):
-        return remote(crecv.at[:, x_at(k), low, :], xr1.at[k - 1],
-                      igx_s.at[0, k], igx_r.at[0, k], at(z, y, x_at(k), c))
-
-    def ig_y1():
-        return remote(crecv.at[yo, x, low, :], yr1, igx_s.at[1, 0], igx_r.at[1, 0], y_dev)
-
-    def ig_y2():
-        return remote(crecv.at[yo, :, high, :], yr2, igx_s.at[2, 0], igx_r.at[2, 0], y_dev)
-
-    def ig_x2(k):
-        return remote(crecv.at[y, x_at(k), high, :], xr2.at[k - 1],
-                      igx_s.at[3, k], igx_r.at[3, k], at(z, y, x_at(k), c))
-
-    def ig_first():
+    def ig_x1(g, k):
+        return remote(crecv.at[:, x_at(k), low, sets[g]], xr1.at[k - 1, :, :, sets[g]],
+                      igx_s.at[g, 0, k], igx_r.at[g, 0, k], at(z, y, x_at(k), c))
+
+    def ig_y1(g):
+        return remote(crecv.at[yo, x, low, sets[g]], yr1.at[:, sets[g]],
+                      igx_s.at[g, 1, 0], igx_r.at[g, 1, 0], y_dev)
+
+    def ig_y2(g):
+        return remote(crecv.at[yo, :, high, sets[g]], yr2.at[:, :, sets[g]],
+                      igx_s.at[g, 2, 0], igx_r.at[g, 2, 0], y_dev)
+
+    def ig_x2(g, k):
+        return remote(crecv.at[y, x_at(k), high, sets[g]], xr2.at[k - 1, :, sets[g]],
+                      igx_s.at[g, 3, k], igx_r.at[g, 3, k], at(z, y, x_at(k), c))
+
+    def ig_first(g):
         for k in range(1, nx):
-            go(ig_x1(k))
-        go(ig_y2())
-
-    def ig_second():
+            go(ig_x1(g, k))
+        go(ig_y2(g))
+
+    def ig_second(g):
         for k in range(1, nx):
-            ig_x1(k).wait_recv()
+            ig_x1(g, k).wait_recv()
         for yy in range(ny):
-            accumulate(crecv.at[yy, x, low, :], [xr1.at[k, yy] for k in range(nx - 1)])
-        go(ig_y1())
-        ig_y2().wait_recv()
+            accumulate(crecv.at[yy, x, low, sets[g]],
+                       [xr1.at[k, yy, :, sets[g]] for k in range(nx - 1)])
+        go(ig_y1(g))
+        ig_y2(g).wait_recv()
         for xx in range(nx):
-            accumulate(crecv.at[y, xx, high, :], [yr2.at[xx]])
+            accumulate(crecv.at[y, xx, high, sets[g]], [yr2.at[xx, :, sets[g]]])
         for k in range(1, nx):
-            go(ig_x2(k))
-
-    ig_local = pltpu.make_async_copy(crecv.at[y, x], ig_out, loc.at[5])
-
-    def ig_last():
-        ig_y1().wait_recv()
-        accumulate(crecv.at[y, x, low, :], [yr1])
+            go(ig_x2(g, k))
+
+    ig_local = [
+        pltpu.make_async_copy(crecv.at[y, x, :, sets[g]], ig_out.at[:, sets[g]], loc.at[5 + g])
+        for g in range(2)
+    ]
+
+    def ig_last(g):
+        ig_y1(g).wait_recv()
+        accumulate(crecv.at[y, x, low, sets[g]], [yr1.at[:, sets[g]]])
         for k in range(1, nx):
-            ig_x2(k).wait_recv()
-        accumulate(crecv.at[y, x, high, :], [xr2.at[k] for k in range(nx - 1)])
-        ig_local.start()
+            ig_x2(g, k).wait_recv()
+        accumulate(crecv.at[y, x, high, sets[g]],
+                   [xr2.at[k, :, sets[g]] for k in range(nx - 1)])
+        ig_local[g].start()
 
     def acts_in(index):
         act_copy(index, True).wait_recv()
 
     def start():
-        ag_step(DN, 0, 0)
-        og_rows.start_y()
-        og_rows.start_x()
+        ag_step(DN, 0, 0, 0)
+        for p in order[:2]:
+            og_rows.start_y(p)
+            og_rows.start_x(p)
+        go(act_copy(0))
         go(weight_y(DN))
-        go(act_copy(0))
+        for p in order[2:]:
+            og_rows.start_y(p)
         go(act_copy(1))
         go(weight_y(UP))
         go(act_copy(2))
+        in_rows.start_y(0)
         go(act_copy(3))
-        in_rows.start_y()
-        ag_step(UP, 0, 0, "edge")
+        ag_step(UP, 0, 0, 0, "edge")
+        ag_step(UP, 0, 1, 0, "edge")
         for copy in local:
             copy.start()
+
+    def first_rows():
+        for p in order[:2]:
+            og_rows.relay_y(p)
+            og_rows.relay_x(p, 0)
+        for p in order[2:]:
+            og_rows.start_x(p)
+
+    def first_rows_in():
+        for p in order[:2]:
+            og_rows.relay_x(p, 1)
+        for p in order[:2]:
+            og_rows.finish(p)
+
+    def more_rows(p):
+        og_rows.relay_y(p)
+        og_rows.relay_x(p, 0)
+
+    def more_rows_in(p):
+        og_rows.relay_x(p, 1)
+        og_rows.finish(p)
 
     def local_wait():
         for copy in local:
@@ -486,90 +567,118 @@
         weight_y(w, True).wait_recv()
 
     def ig_drain():
-        @pl.loop(0, ny * nx)
-        def _(j):
-            ig_c(j).wait_send()
-        ig_local.wait()
-
-    def steps(function, *args, first=2):
-        return [(function, *args, k) for k in range(first, nz - 1)]
+        for g in range(2):
+            @pl.loop(0, ny * nx)
+            def _(j):
+                ig_c(g, j).wait_send()
+            ig_local[g].wait()
+
+    def gather_on(w, u, h):
+        near_steps = [(ag_step, w, u, h, k, "near") for k in range(2, nz // 2)]
+        return near_steps + [(ag_step, w, u, h, k, "far") for k in range(2, nz - 1)]
 
     plan = [
         (start,),
-        (ag_step, DN, 0, 1),
-        (og_rows.relay_y,),
-        (og_rows.relay_x, 0),
-        (in_rows.start_x,),
-        *steps(ag_step, DN, 0),
-        (weight_in, DN),
-        (ag_step, DN, 1, 0),
-        (og_rows.relay_x, 1),
-        (og_rows.finish,),
+        (first_rows,),
+        (ag_step, DN, 0, 0, 1),
+        (first_rows_in,),
         (local_wait,),
         (acts_in, 0),
         (squares, 0),
-        (dot_dn, 0),
-        (ag_step, DN, 1, 1),
+        (dot_dn, 0, 0, 2),
+        *gather_on(DN, 0, 0),
+        (weight_in, DN),
+        (ag_step, DN, 1, 0, 0),
+        (near, DN, 0, 0, 1),
+        *[(more_rows, p) for p in order[2:]],
+        (in_rows.start_x, 0),
+        *[call for i, p in enumerate(order[2:])
+          for call in ((more_rows_in, p), (dot_dn, 0, i + 2, i + 3))],
+        (ag_step, DN, 1, 0, 1),
         (acts_in, 1),
         (squares, 1),
         (dot_dn, 1),
-        (near, DN, 0),
-        *steps(ag_step, DN, 1),
-        (ag_step, UP, 0, 0, "inner"),
+        (near, DN, 0, 1, nz - 2),
+        *gather_on(DN, 1, 0),
         (weight_in, UP),
-        (far, DN, 0),
+        (ag_step, UP, 1, 0, 0, "edge"),
+        (ag_step, UP, 1, 1, 0, "edge"),
+        (ag_step, UP, 0, 0, 0, "inner"),
+        (ag_step, UP, 1, 0, 0, "inner"),
+        (ag_step, UP, 0, 0, 1, "near"),
         (acts_in, 2),
         (squares, 2),
         (dot_dn, 2),
         (near, DN, 1),
-        (ag_step, UP, 0, 1),
+        (ag_step, UP, 0, 0, 1, "far"),
+        (ag_step, UP, 1, 0, 1, "near"),
+        (ag_finish, DN, 0, 0),
+        (ag_finish, DN, 1, 0),
+        (dot_hg, 0),
+        (dot_hg, 1),
+        (dot_hg, 2),
+        (ag_step, UP, 1, 0, 1, "far"),
+        (ag_step, UP, 0, 1, 0, "inner"),
+        (ag_step, UP, 1, 1, 0, "inner"),
+        (ag_step, UP, 0, 1, 1, "near"),
+        (ag_step, UP, 1, 1, 1, "near"),
+        (in_rows.relay_y, 0),
+        (in_rows.relay_x, 0, 0),
+        *gather_on(UP, 0, 0),
+        *gather_on(UP, 1, 0),
         (acts_in, 3),
         (squares, 3),
         (dot_dn, 3),
-        (ag_finish, DN, 0),
-        (ag_finish, DN, 1),
-        (dot_hg,),
+        (dot_hg, 3),
         (near, DN, 2),
+        (in_rows.relay_x, 0, 1),
+        (in_rows.finish, 0),
+        (dot_up, 0),
+        (ag_step, UP, 0, 1, 1, "far"),
+        (dot_up, 1),
+        (near, DN, 3),
+        (ag_step, UP, 1, 1, 1, "far"),
+        (ag_finish, UP, 0, 0),
+        (ag_finish, UP, 1, 0),
+        (og_rows.drain,),
+        (dot_in, 0, True),
+        *gather_on(UP, 0, 1),
+        (dot_in, 0, False),
+        (dot_up, 2),
+        *gather_on(UP, 1, 1),
+        (ig_sum, 0),
+        (ig_first, 0),
+        (dot_up, 3),
+        (far, DN, 0),
         (far, DN, 1),
-        *steps(ag_step, UP, 0),
-        (ag_step, UP, 1, 0),
-        (in_rows.relay_y,),
-        (in_rows.relay_x, 0),
-        (near, DN, 3),
+        (near, UP, 0),
+        (ig_second, 0),
+        (ag_finish, UP, 0, 1),
+        (ag_finish, UP, 1, 1),
+        (dot_in, 1, True),
+        (dot_in, 1, False),
         (far, DN, 2),
-        (ag_step, UP, 1, 1),
-        (in_rows.relay_x, 1),
-        (in_rows.finish,),
-        (dot_up, 0),
         (far, DN, 3),
-        *steps(ag_step, UP, 1),
-        (dot_up, 1),
-        (dot_up, 2),
-        (dot_up, 3),
-        (near, UP, 0),
+        (ig_sum, 1),
+        (ig_first, 1),
+        (far, UP, 0),
+        (near, UP, 1),
+        (ig_last, 0),
         (rs_finish, DN, 0),
         (rs_finish, DN, 1),
-        (far, UP, 0),
-        (near, UP, 1),
+        (far, UP, 1),
+        (ig_second, 1),
         (rs_finish, DN, 2),
         (rs_finish, DN, 3),
-        (ag_finish, UP, 0),
-        (ag_finish, UP, 1),
-        (og_rows.drain,),
-        (dot_in, True),
-        (far, UP, 1),
         (near, UP, 2),
-        (dot_in, False),
-        (ig_sum,),
-        (ig_first,),
+        (ig_last, 1),
+        (far, UP, 2),
         (rs_finish, UP, 0),
-        (far, UP, 2),
-        (near, UP, 3),
+        (near, UP, 3, 0, 1),
         (rs_finish, UP, 1),
+        (near, UP, 3, 1, nz - 2),
         (far, UP, 3),
-        (ig_second,),
         (rs_finish, UP, 2),
-        (ig_last,),
         (rs_finish, UP, 3),
         (in_rows.drain,),
         (drain, sends),
@@ -608,6 +717,7 @@
             vm((m.all_rows, m.d), BF16),
             vm((m.all_rows, m.hh), BF16),
             vm((m.all_rows, m.hh), BF16),
+            vm((m.all_rows, m.hh), BF16),
             vm((m.hh, m.d), BF16),
             vm((m.d, m.hh), BF16),
             vm((m.nz, CHUNKS, m.hc, m.dz), BF16),
@@ -619,13 +729,13 @@
             vm((m.half, m.d), BF16),
             vm((m.nx, m.half, m.d), BF16),
             vm((m.nx - 1, m.half, m.d), BF16),
-            dma((6,)),
-            dma((2, m.ny, 2, m.nz - 1)),
-            dma((2, m.ny, 2, m.nz - 1)),
+            dma((7,)),
+            dma((2, m.ny, 2, 2, m.nz - 1)),
+            dma((2, m.ny, 2, 2, m.nz - 1)),
             dma((2,)),
             dma((2,)),
-            dma((2, rows_events)),
-            dma((2, rows_events)),
+            dma((2, rows_events * m.nz)),
+            dma((2, rows_events * m.nz)),
             dma((ACT_PARTS,)),
             dma((ACT_PARTS,)),
             dma((2, 2, m.nz, CHUNKS)),
@@ -633,16 +743,17 @@
             dma((2, CHUNKS)),
             dma((2, CHUNKS)),
             dma((2, CHUNKS)),
-            dma((m.ny * m.nx,)),
-            dma((m.ny * m.nx,)),
-            dma((4, m.nx)),
-            dma((4, m.nx)),
+            dma((2, m.ny * m.nx)),
+            dma((2, m.ny * m.nx)),
+            dma((2, 4, m.nx)),
+            dma((2, 4, m.nx)),
         ],
         cost_estimate=pl.CostEstimate(flops=flops, bytes_accessed=2**25, transcendentals=0),
         compiler_params=pltpu.CompilerParams(
             collective_id=0, has_side_effects=True, vmem_limit_bytes=67043328
         ),
     )(inp, act, og, upw, dnw)
+    ig = ig.reshape(m.t, 2, m.fs, m.df // 2).transpose(0, 2, 1, 3).reshape(m.t, m.d)
     return ig, ug.astype(F32), dg.astype(F32)
 
 

time: 229 us -> 213 us (0.930)
  Pallas kernels: 220 us -> 204 us
  local copies, waits for them, and re-layouts: 0.89 us -> 3.67 us
    pallas_call x1, Pallas kernels: 220 us -> 204 us  [local_step(): pl.pallas_call(functools.partial(kernel, m), name='ffn_backward', out_sha...]
where the time goes in v2:
time: 213 us; the launch traced here: 211 us
  Pallas kernels  204 us (96%)
  local copies, waits for them, and re-layouts  3.67 us (2%)
  other arithmetic  3.04 us (1%)
    pallas_call x1, Pallas kernels, local_step(): pl.pallas_call(functools.partial(kernel, m), name='ffn_backward', out_sha...  204 us

profile of v2, /device:TPU:8, one launch (start us, length us, event | category | flops | bytes accessed | tf_op | source)
XLA Modules:
  0.0 211.0 jit_solution(16351690641219692803)
XLA Ops:
  0.6 203.7 %ffn_backward.1 = (bf16[192,2048]{1,0:T(8,128)(2,1)}, bf16[256,2048]{1,0:T(8,128)(2,1)}, bf16[2048,256]{1,0:T(8,128)(2,1)}) custom-call(bf16[192,2048]{1,0:T(8,128)(2,1)} %inp.1, bf16[768,2048]{1,0:T(8,128)(2,1)} %act.1, bf16[192,2048]{1,0:T(8,128)(2,1)} %og.1, bf16[256,2048]{1,0:T(8,128)(2,1)} %upw.1, bf16[2048,256]{1,0:T(8,128)(2,1)} %dnw.1), custom_call_target="tpu_custom_call" | custom-call | flops 25769803776 | bytes 33554432 | tf_op jit(solution)/shard_map/ffn_backward/pallas_call | solution.py:705
  204.3 0.0 copy-start.1
  204.3 1.4 copy.9
  205.7 0.8 copy.8
  206.5 0.0 copy-start
  206.5 1.5 reshape.13
  208.0 0.0 copy-done.1
  208.0 1.6 convert_element_type.6
  209.6 0.0 copy-done
  209.6 1.5 convert_element_type.7
Async XLA Ops:
  204.3 3.7 %copy-start.1 = (bf16[256,2048]{1,0:T(8,128)(2,1)S(1)}, bf16[256,2048]{1,0:T(8,128)(2,1)}, u32[]{:S(2)}) copy-start(bf16[256,2048]{1,0:T(8,128)(2,1)} %get-tuple-element.7) | copy-start | bytes 3145732
  206.5 3.0 %copy-start = (bf16[2048,256]{1,0:T(8,128)(2,1)S(1)}, bf16[2048,256]{1,0:T(8,128)(2,1)}, u32[]{:S(2)}) copy-start(bf16[2048,256]{1,0:T(8,128)(2,1)} %get-tuple-element.8) | copy-start | bytes 3145732

commit v3 on v2

--- a/solution.py
+++ b/solution.py
@@ -33,6 +33,7 @@
         self.half = tokens // 2
         self.hc = self.hh // CHUNKS
         self.ha = self.hh // ACT_PARTS
+        self.direct = (self.df // 2) % 128 == 0
 
 
 def kernel(
@@ -58,6 +59,11 @@
 
     def x_at(k):
         return lax.rem(x + k, nx)
+
+    def mirror(target):
+        return jnp.where(z < nz // 2, target, nz - 1 - target)
+
+    order = [mirror(nz - 1 - i // 2 if i % 2 == 0 else i // 2) for i in range(nz)]
 
     def remote(src, dst, ss, rs, dev):
         return pltpu.make_async_remote_copy(
@@ -169,12 +175,15 @@
         def drain(self):
             drain(self.sends)
 
+        def cols(self, p):
+            return pl.ds(aligned(p * self.width, self.width), self.width)
+
         def src(self, p):
-            return self.source.at[:, pl.ds(p * self.width, self.width)]
+            return self.source.at[:, self.cols(p)]
 
         def place(self, p, yy, xx, cc):
             start = aligned(((yy * nx + xx) * 2 + cc) * m.t, m.t)
-            return self.buf.at[pl.ds(start, m.t), pl.ds(p * self.width, self.width)]
+            return self.buf.at[pl.ds(start, m.t), self.cols(p)]
 
         def copy(self, p, index, src, where, dev):
             index = index * self.pieces + p
@@ -233,13 +242,13 @@
         return remote(src, dst, act_s.at[part], act_r.at[part], y_dev)
 
     local = [
-        pltpu.make_async_copy(weight_own(DN, y), weight_view(DN, f), loc.at[0]),
-        pltpu.make_async_copy(weight_own(UP, y), weight_view(UP, f), loc.at[1]),
-        pltpu.make_async_copy(og, slot(og_all, y, x, c), loc.at[2]),
-        pltpu.make_async_copy(inp, slot(in_all, y, x, c), loc.at[3]),
+        pltpu.make_async_copy(weight_own(DN, y), weight_view(DN, f), loc.at[0, 0]),
+        pltpu.make_async_copy(weight_own(UP, y), weight_view(UP, f), loc.at[1, 0]),
+        pltpu.make_async_copy(og, slot(og_all, y, x, c), loc.at[2, 0]),
+        pltpu.make_async_copy(inp, slot(in_all, y, x, c), loc.at[3, 0]),
         pltpu.make_async_copy(
             act.at[:, pl.ds(aligned(y * m.hh, m.hh), m.hh)],
-            acts.at[pl.ds(aligned(y * m.rows, m.rows), m.rows), :], loc.at[4]),
+            acts.at[pl.ds(aligned(y * m.rows, m.rows), m.rows), :], loc.at[4, 0]),
     ]
 
     parts, slots = (part_dn, part_up), (slot_dn, slot_up)
@@ -366,9 +375,7 @@
 
     def targets(i):
         turn = i // 2
-        return jnp.where(i % 2 == 0, nz - 1 - turn, turn)
-
-    order = [nz - 1 - i // 2 if i % 2 == 0 else i // 2 for i in range(nz)]
+        return mirror(jnp.where(i % 2 == 0, nz - 1 - turn, turn))
 
     def squares(ch):
         cols = pl.ds(ch * m.hc, m.hc)
@@ -403,14 +410,21 @@
             grad = dot_cols(og_all[rows, :], dn_all[cols, :])
             pre[rows, cols] = (2.0 * active * grad).astype(BF16)
 
-    def dot_up(ch):
+    def dot_up(ch, send=True):
         @pl.loop(0, nz)
         def _(i):
             target = targets(i)
             a = in_all[:, pl.ds(aligned(target * m.dz, m.dz), m.dz)]
             b = pre[:, pl.ds(ch * m.hc, m.hc)]
             part_up[target, ch] = dot_rows(a, b).astype(BF16)
-            rs_edge(UP, target, ch)
+            if send:
+                rs_edge(UP, target, ch)
+
+    def up_sends(first):
+        @pl.loop(0, nz * (CHUNKS - first))
+        def _(i):
+            count = CHUNKS - first
+            rs_edge(UP, targets(i // count), first + i % count)
 
     part = og_all
     width = m.d // 2
@@ -502,10 +516,19 @@
         for k in range(1, nx):
             go(ig_x2(g, k))
 
-    ig_local = [
-        pltpu.make_async_copy(crecv.at[y, x, :, sets[g]], ig_out.at[:, sets[g]], loc.at[5 + g])
-        for g in range(2)
-    ]
+    piece = m.df // 2
+
+    def ig_local(g):
+        mine = crecv.at[y, x]
+        if not m.direct:
+            return [pltpu.make_async_copy(mine.at[:, sets[g]], ig_out.at[:, sets[g]],
+                                          loc.at[5 + g, 0])]
+        return [
+            pltpu.make_async_copy(
+                mine.at[:, pl.ds(g * width + n * piece, piece)],
+                ig_out.at[:, pl.ds(n * m.df + g * piece, piece)], loc.at[5 + g, n])
+            for n in range(m.fs)
+        ]
 
     def ig_last(g):
         ig_y1(g).wait_recv()
@@ -514,7 +537,8 @@
             ig_x2(g, k).wait_recv()
         accumulate(crecv.at[y, x, high, sets[g]],
                    [xr2.at[k, :, sets[g]] for k in range(nx - 1)])
-        ig_local[g].start()
+        for copy in ig_local(g):
+            copy.start()
 
     def acts_in(index):
         act_copy(index, True).wait_recv()
@@ -533,8 +557,8 @@
         go(act_copy(2))
         in_rows.start_y(0)
         go(act_copy(3))
-        ag_step(UP, 0, 0, 0, "edge")
-        ag_step(UP, 0, 1, 0, "edge")
+        ag_step(UP, 0, 0, 0)
+        ag_step(UP, 0, 1, 0)
         for copy in local:
             copy.start()
 
@@ -571,7 +595,8 @@
             @pl.loop(0, ny * nx)
             def _(j):
                 ig_c(g, j).wait_send()
-            ig_local[g].wait()
+            for copy in ig_local(g):
+                copy.wait()
 
     def gather_on(w, u, h):
         near_steps = [(ag_step, w, u, h, k, "near") for k in range(2, nz // 2)]
@@ -603,7 +628,6 @@
         (weight_in, UP),
         (ag_step, UP, 1, 0, 0, "edge"),
         (ag_step, UP, 1, 1, 0, "edge"),
-        (ag_step, UP, 0, 0, 0, "inner"),
         (ag_step, UP, 1, 0, 0, "inner"),
         (ag_step, UP, 0, 0, 1, "near"),
         (acts_in, 2),
@@ -618,7 +642,6 @@
         (dot_hg, 1),
         (dot_hg, 2),
         (ag_step, UP, 1, 0, 1, "far"),
-        (ag_step, UP, 0, 1, 0, "inner"),
         (ag_step, UP, 1, 1, 0, "inner"),
         (ag_step, UP, 0, 1, 1, "near"),
         (ag_step, UP, 1, 1, 1, "near"),
@@ -644,11 +667,12 @@
         (dot_in, 0, True),
         *gather_on(UP, 0, 1),
         (dot_in, 0, False),
-        (dot_up, 2),
+        (dot_up, 2, False),
         *gather_on(UP, 1, 1),
         (ig_sum, 0),
         (ig_first, 0),
-        (dot_up, 3),
+        (dot_up, 3, False),
+        (up_sends, 2),
         (far, DN, 0),
         (far, DN, 1),
         (near, UP, 0),
@@ -670,11 +694,12 @@
         (ig_second, 1),
         (rs_finish, DN, 2),
         (rs_finish, DN, 3),
-        (near, UP, 2),
+        (near, UP, 2, 0, 1),
         (ig_last, 1),
+        (near, UP, 3, 0, 1),
+        (rs_finish, UP, 0),
+        (near, UP, 2, 1, nz - 2),
         (far, UP, 2),
-        (rs_finish, UP, 0),
-        (near, UP, 3, 0, 1),
         (rs_finish, UP, 1),
         (near, UP, 3, 1, nz - 2),
         (far, UP, 3),
@@ -689,7 +714,7 @@
         (fin_wait, UP),
     ]
     for index, (function, *args) in enumerate(plan):
-        tags = [str(arg) for arg in args if not isinstance(arg, list)]
+        tags = [str(arg) for arg in args if isinstance(arg, (int, str))]
         label = "_".join([str(index), function.__name__, *tags])
         with jax.named_scope(label):
             function(*args)
@@ -729,7 +754,7 @@
             vm((m.half, m.d), BF16),
             vm((m.nx, m.half, m.d), BF16),
             vm((m.nx - 1, m.half, m.d), BF16),
-            dma((7,)),
+            dma((7, m.fs)),
             dma((2, m.ny, 2, 2, m.nz - 1)),
             dma((2, m.ny, 2, 2, m.nz - 1)),
             dma((2,)),
@@ -753,7 +778,9 @@
             collective_id=0, has_side_effects=True, vmem_limit_bytes=67043328
         ),
     )(inp, act, og, upw, dnw)
-    ig = ig.reshape(m.t, 2, m.fs, m.df // 2).transpose(0, 2, 1, 3).reshape(m.t, m.d)
+    if not m.direct:
+        ig = ig.reshape(m.t, 2, m.fs, m.df // 2).transpose(0, 2, 1, 3)
+        ig = ig.reshape(m.t, m.d)
     return ig, ug.astype(F32), dg.astype(F32)
 
 

time: 213 us -> 202 us (0.948)
  Pallas kernels: 204 us -> 195 us
  local copies, waits for them, and re-layouts: 3.67 us -> 0.89 us
    pallas_call x1, Pallas kernels: 204 us -> 195 us  [local_step(): pl.pallas_call(functools.partial(kernel, m), name='ffn_backward', out_sha...]
where the time goes in v3:
time: 202 us; the launch traced here: 200 us
  Pallas kernels  195 us (97%)
  other arithmetic  4.36 us (2%)
    pallas_call x1, Pallas kernels, local_step(): pl.pallas_call(functools.partial(kernel, m), name='ffn_backward', out_sha...  195 us
    convert_element_type x2, other arithmetic, local_step(): return (ig, ug.astype(F32), dg.astype(F32))  4.36 us

profile of v3, /device:TPU:8, one launch (start us, length us, event | category | flops | bytes accessed | tf_op | source)
XLA Modules:
  0.0 200.5 jit_solution(4992197118423538297)
XLA Ops:
  0.6 194.6 %ffn_backward.1 = (bf16[192,2048]{1,0:T(8,128)(2,1)}, bf16[256,2048]{1,0:T(8,128)(2,1)}, bf16[2048,256]{1,0:T(8,128)(2,1)}) custom-call(bf16[192,2048]{1,0:T(8,128)(2,1)} %inp.1, bf16[768,2048]{1,0:T(8,128)(2,1)} %act.1, bf16[192,2048]{1,0:T(8,128)(2,1)} %og.1, bf16[256,2048]{1,0:T(8,128)(2,1)} %upw.1, bf16[2048,256]{1,0:T(8,128)(2,1)} %dnw.1), custom_call_target="tpu_custom_call" | custom-call | flops 25769803776 | bytes 33554432 | tf_op jit(solution)/shard_map/ffn_backward/pallas_call | solution.py:730
  195.2 0.0 copy-start
  195.2 2.9 %convert_element_type.6 = f32[256,2048]{1,0:T(8,128)} convert(bf16[256,2048]{1,0:T(8,128)(2,1)} %get-tuple-element.7) | non-fusion elementwise | flops 524288 | bytes 3145728 | tf_op jit(solution)/shard_map/convert_element_type | solution.py:784
  198.1 0.0 copy-done
  198.1 0.0 copy-start.1
  198.1 1.5 convert_element_type.7
  199.6 0.0 copy-done.1
  199.6 0.9 copy.9
Async XLA Ops:
  195.2 2.9 %copy-start = (bf16[2048,256]{1,0:T(8,128)(2,1)S(1)}, bf16[2048,256]{1,0:T(8,128)(2,1)}, u32[]{:S(2)}) copy-start(bf16[2048,256]{1,0:T(8,128)(2,1)} %get-tuple-element.8) | copy-start | bytes 3145732
  198.1 1.5 copy-start.1

commit v4 on v3

--- a/solution.py
+++ b/solution.py
@@ -41,7 +41,7 @@
     og_all, in_all, acts, hid, pre, dn_all, up_all,
     part_dn, part_up, slot_dn, slot_up, crecv, xr1, yr1, yr2, xr2,
     loc, ag_s, ag_r, wy_s, wy_r, tok_s, tok_r, act_s, act_r,
-    rs_s, rs_r, fin_s, fin_r, fin_l, igc_s, igc_r, igx_s, igx_r,
+    rs_s, rs_r, fin_s, fin_r, igc_s, igc_r, igx_s, igx_r,
 ):
     f, tt = lax.axis_index("fs"), lax.axis_index("tp")
     ny, nx, nz = m.ny, m.nx, m.nz
@@ -127,8 +127,8 @@
         origin = jnp.clip(z - back if side == RIGHT else z + back, 0, nz - 1)
         view = weight_view(w, origin * ny + (y if u == 0 else yo), h)
         src = weight_own(w, y, h) if (u == 0 and k == 0) else view
-        return remote(src, view, ag_s.at[w, u, h, side, k], ag_r.at[w, u, h, side, k],
-                      z_dev[side])
+        unit = u if w == DN else ny + 2 * u + h
+        return remote(src, view, ag_s.at[unit, side, k], ag_r.at[unit, origin], z_dev[side])
 
     def ag_sends(side, k):
         if side == RIGHT:
@@ -166,14 +166,13 @@
 
     class Rows:
         def __init__(self, a, src, buf, pieces):
-            self.a, self.buf, self.sends = a, buf, []
+            self.a, self.buf = a, buf
             self.pieces, self.width, self.source = pieces, m.d // pieces, src
 
-        def go(self, copy):
-            go(copy, None, self.sends)
-
         def drain(self):
-            drain(self.sends)
+            count = 4 * nx - 1
+            every = self.buf.at[pl.ds(0, count * m.t), :]
+            remote(every, every, tok_s.at[self.a], tok_r.at[nz, 0], y_dev).wait_send()
 
         def cols(self, p):
             return pl.ds(aligned(p * self.width, self.width), self.width)
@@ -186,9 +185,9 @@
             return self.buf.at[pl.ds(start, m.t), self.cols(p)]
 
         def copy(self, p, index, src, where, dev):
-            index = index * self.pieces + p
-            return remote(src, self.place(p, *where), tok_s.at[self.a, index],
-                          tok_r.at[self.a, index], dev)
+            row = p if self.a == 0 else nz
+            return remote(src, self.place(p, *where), tok_s.at[self.a],
+                          tok_r.at[row, index], dev)
 
         def over_y(self, p, receive=False):
             return self.copy(p, 0, self.src(p), (yo if receive else y, x, c), y_dev)
@@ -200,36 +199,35 @@
             index = 1 + j * (nx - 1) + k - 1
             return self.copy(p, index, src, (yy, xx, c), at(z, y, x_at(k), c))
 
-        def over_c(self, p, j, k, receive=False):
+        def over_c(self, p, j, k):
             yy = y if j == 0 else yo
             xx = x_at(nx - k) if k else x
             src = self.src(p) if j == 0 and k == 0 else self.place(p, yy, xx, c)
-            index = 1 + 2 * (nx - 1) + j * nx + k
-            return self.copy(p, index, src, (yy, xx, co if receive else c), c_dev)
+            return self.copy(p, 2 * nx - 1, src, (yy, xx, c), c_dev)
 
         def start_y(self, p):
-            self.go(self.over_y(p))
+            self.over_y(p).start()
 
         def start_x(self, p):
             for k in range(1, nx):
-                self.go(self.over_x(p, 0, k))
-            self.go(self.over_c(p, 0, 0))
+                self.over_x(p, 0, k).start()
+            self.over_c(p, 0, 0).start()
 
         def relay_y(self, p):
             self.over_y(p, True).wait_recv()
             for k in range(1, nx):
-                self.go(self.over_x(p, 1, k))
-            self.go(self.over_c(p, 1, 0))
+                self.over_x(p, 1, k).start()
+            self.over_c(p, 1, 0).start()
 
         def relay_x(self, p, j):
             for k in range(1, nx):
                 self.over_x(p, j, k, True).wait_recv()
-                self.go(self.over_c(p, j, k))
+                self.over_c(p, j, k).start()
 
         def finish(self, p):
-            for j in range(ny):
-                for k in range(nx):
-                    self.over_c(p, j, k, True).wait_recv()
+            row = p if self.a == 0 else nz
+            half = self.buf.at[pl.ds(0, 2 * nx * m.t), self.cols(p)]
+            remote(half, half, tok_s.at[self.a], tok_r.at[row, 2 * nx - 1], c_dev).wait_recv()
 
     og_rows = Rows(0, og, og_all, nz)
     in_rows = Rows(1, inp, in_all, 1)
@@ -239,16 +237,16 @@
         src = act.at[:, pl.ds(aligned(yo * m.hh + col, m.ha), m.ha)]
         row = aligned((yo if receive else y) * m.rows, m.rows)
         dst = acts.at[pl.ds(row, m.rows), pl.ds(col, m.ha)]
-        return remote(src, dst, act_s.at[part], act_r.at[part], y_dev)
+        return remote(src, dst, act_s, act_r.at[part], y_dev)
 
     local = [
-        pltpu.make_async_copy(weight_own(DN, y), weight_view(DN, f), loc.at[0, 0]),
-        pltpu.make_async_copy(weight_own(UP, y), weight_view(UP, f), loc.at[1, 0]),
-        pltpu.make_async_copy(og, slot(og_all, y, x, c), loc.at[2, 0]),
-        pltpu.make_async_copy(inp, slot(in_all, y, x, c), loc.at[3, 0]),
+        pltpu.make_async_copy(weight_own(DN, y), weight_view(DN, f), loc.at[0]),
+        pltpu.make_async_copy(weight_own(UP, y), weight_view(UP, f), loc.at[1]),
+        pltpu.make_async_copy(og, slot(og_all, y, x, c), loc.at[2]),
+        pltpu.make_async_copy(inp, slot(in_all, y, x, c), loc.at[3]),
         pltpu.make_async_copy(
             act.at[:, pl.ds(aligned(y * m.hh, m.hh), m.hh)],
-            acts.at[pl.ds(aligned(y * m.rows, m.rows), m.rows), :], loc.at[4, 0]),
+            acts.at[pl.ds(aligned(y * m.rows, m.rows), m.rows), :], loc.at[4]),
     ]
 
     parts, slots = (part_dn, part_up), (slot_dn, slot_up)
@@ -259,13 +257,12 @@
             place = target
         else:
             place = jnp.where(target == z - 1, nz, target)
-        return remote(src, slots[w].at[place, ch], rs_s.at[w, side, target, ch],
-                      rs_r.at[w, side, target, ch], z_dev[side])
-
-    def rs_waits(w, side, target, ch, place):
-        return remote(parts[w].at[0, ch], slots[w].at[place, ch],
-                      rs_s.at[w, side, target, ch], rs_r.at[w, side, target, ch],
-                      z_dev[side])
+        return remote(src, slots[w].at[place, ch], rs_s.at[w, target],
+                      rs_r.at[w, place, ch], z_dev[side])
+
+    def rs_waits(w, side, ch, place):
+        return remote(parts[w].at[0, ch], slots[w].at[place, ch], rs_s.at[w, 0],
+                      rs_r.at[w, place, ch], z_dev[side])
 
     def by_rows(count, step, body):
         @pl.loop(0, count // step)
@@ -290,7 +287,7 @@
 
         @pl.when(cond)
         def _():
-            rs_waits(w, side, target, ch, target).wait_recv()
+            rs_waits(w, side, ch, target).wait_recv()
             buf, own = slots[w].at[target, ch], parts[w].at[target, ch]
 
             def add(rows):
@@ -323,55 +320,58 @@
 
     def rs_drain(w):
         for target in range(nz):
-            @pl.loop(0, CHUNKS)
-            def _(ch):
-                pl.when(z < target)(rs(w, RIGHT, target, ch, False).wait_send)
-                pl.when(z > target)(rs(w, LEFT, target, ch, False).wait_send)
-
-    def fin_copy(w, ch, yy, receive=False):
-        src = parts[w].at[z, ch]
+            every = slots[w].at[target]
+            pl.when(z != target)(
+                remote(every, every, rs_s.at[w, target], rs_r.at[w, 0, 0], y_dev).wait_send)
+
+    def fin_cut(w, buf, yy):
+        cut = pl.ds(aligned(yy * m.df, m.df), m.df)
+        return buf.at[:, cut] if w == DN else buf.at[cut, :]
+
+    def fin_place(w, ch, yy):
+        start = aligned(yy * m.hh + ch * m.hc, m.hc)
         if w == DN:
-            src = src.at[:, pl.ds(aligned(yy * m.df, m.df), m.df)]
-            row = aligned((yo if receive else y) * m.hh + ch * m.hc, m.hc)
-            return src, dg_out.at[pl.ds(row, m.hc), :]
-        src = src.at[pl.ds(aligned(yy * m.df, m.df), m.df), :]
-        col = aligned((yo if receive else y) * m.hh + ch * m.hc, m.hc)
-        return src, ug_out.at[:, pl.ds(col, m.hc)]
-
-    def fin_remote(w, ch, receive=False):
-        src, dst = fin_copy(w, ch, yo, receive)
-        return remote(src, dst, fin_s.at[w, ch], fin_r.at[w, ch], y_dev)
-
-    def fin_local(w, ch):
-        src, dst = fin_copy(w, ch, y)
-        return pltpu.make_async_copy(src, dst, fin_l.at[w, ch])
+            return dg_out.at[pl.ds(start, m.hc), :]
+        return ug_out.at[:, pl.ds(start, m.hc)]
+
+    def fin_remote(w, ch):
+        return remote(fin_cut(w, parts[w].at[z, ch], yo), fin_place(w, ch, y),
+                      fin_s.at[w], fin_r.at[w], y_dev)
 
     def rs_finish(w, ch):
         own = parts[w].at[z, ch]
         right, left = slots[w].at[z, ch], slots[w].at[nz, ch]
-        pl.when(z > 0)(rs_waits(w, RIGHT, z, ch, z).wait_recv)
-        pl.when(z < nz - 1)(rs_waits(w, LEFT, z, ch, nz).wait_recv)
-
-        def total(*others):
+        pl.when(z > 0)(rs_waits(w, RIGHT, ch, z).wait_recv)
+        pl.when(z < nz - 1)(rs_waits(w, LEFT, ch, nz).wait_recv)
+
+        def total(yy, dst, others):
+            terms = [fin_cut(w, buf, yy) for buf in others]
+
             def add(rows):
-                value = own[rows, :].astype(F32)
-                for other in others:
-                    value = value + other[rows, :].astype(F32)
-                own[rows, :] = value.astype(BF16)
-            by_rows(own.shape[0], 64, add)
-
-        pl.when(z == 0)(lambda: total(left))
-        pl.when(z == nz - 1)(lambda: total(right))
-        pl.when(jnp.logical_and(z > 0, z < nz - 1))(lambda: total(right, left))
+                value = terms[0][rows, :].astype(F32)
+                for term in terms[1:]:
+                    value = value + term[rows, :].astype(F32)
+                dst[rows, :] = value.astype(BF16)
+            by_rows(terms[0].shape[0], 64, add)
+
+        def both(yy, dst):
+            pl.when(z == 0)(lambda: total(yy, dst, (own, left)))
+            pl.when(z == nz - 1)(lambda: total(yy, dst, (own, right)))
+            pl.when(jnp.logical_and(z > 0, z < nz - 1))(
+                lambda: total(yy, dst, (own, right, left)))
+
+        both(yo, fin_cut(w, own, yo))
         fin_remote(w, ch).start()
-        fin_local(w, ch).start()
+        both(y, fin_place(w, ch, y))
 
     def fin_wait(w):
-        @pl.loop(0, CHUNKS)
-        def _(ch):
-            fin_remote(w, ch).wait_send()
-            fin_remote(w, ch, True).wait_recv()
-            fin_local(w, ch).wait()
+        def half(yy):
+            cut = pl.ds(aligned(yy * m.hh, m.hh), m.hh)
+            return dg_out.at[cut, :] if w == DN else ug_out.at[:, cut]
+
+        mine, other = half(y), half(yo)
+        remote(mine, mine, fin_s.at[w], fin_r.at[w], y_dev).wait_send()
+        remote(other, other, fin_s.at[w], fin_r.at[w], y_dev).wait_recv()
 
     def targets(i):
         turn = i // 2
@@ -433,7 +433,7 @@
     def ig_c(g, j):
         yy, xx = j // nx, j % nx
         return remote(slot(part, yy, xx, co).at[:, sets[g]], crecv.at[yy, xx, :, sets[g]],
-                      igc_s.at[g, j], igc_r.at[g, j], c_dev)
+                      igc_s.at[g], igc_r.at[g], c_dev)
 
     def dot_in(g, remote_half):
         piece = m.df // 2
@@ -461,10 +461,15 @@
                     for xx in range(nx):
                         ig_c(g, yy * nx + xx).start()
 
+    def ig_all(g):
+        every = crecv.at[:, :, :, sets[g]]
+        return remote(every, every, igc_s.at[g], igc_r.at[g], c_dev)
+
     def ig_sum(g):
+        ig_all(g).wait_recv()
+
         @pl.loop(0, ny * nx)
         def _(j):
-            ig_c(g, j).wait_recv()
             buf = crecv.at[j // nx, j % nx, :, sets[g]]
             own = slot(part, j // nx, j % nx, c).at[:, sets[g]]
 
@@ -484,19 +489,19 @@
 
     def ig_x1(g, k):
         return remote(crecv.at[:, x_at(k), low, sets[g]], xr1.at[k - 1, :, :, sets[g]],
-                      igx_s.at[g, 0, k], igx_r.at[g, 0, k], at(z, y, x_at(k), c))
+                      igx_s.at[g, k - 1], igx_r.at[g, k - 1], at(z, y, x_at(k), c))
 
     def ig_y1(g):
         return remote(crecv.at[yo, x, low, sets[g]], yr1.at[:, sets[g]],
-                      igx_s.at[g, 1, 0], igx_r.at[g, 1, 0], y_dev)
+                      igx_s.at[g, nx - 1], igx_r.at[g, nx - 1], y_dev)
 
     def ig_y2(g):
         return remote(crecv.at[yo, :, high, sets[g]], yr2.at[:, :, sets[g]],
-                      igx_s.at[g, 2, 0], igx_r.at[g, 2, 0], y_dev)
+                      igx_s.at[g, nx], igx_r.at[g, nx], y_dev)
 
     def ig_x2(g, k):
         return remote(crecv.at[y, x_at(k), high, sets[g]], xr2.at[k - 1, :, sets[g]],
-                      igx_s.at[g, 3, k], igx_r.at[g, 3, k], at(z, y, x_at(k), c))
+                      igx_s.at[g, nx + k], igx_r.at[g, nx + k], at(z, y, x_at(k), c))
 
     def ig_first(g):
         for k in range(1, nx):
@@ -518,27 +523,29 @@
 
     piece = m.df // 2
 
-    def ig_local(g):
-        mine = crecv.at[y, x]
+    def ig_store(rows, g, value):
+        value = value.astype(BF16)
         if not m.direct:
-            return [pltpu.make_async_copy(mine.at[:, sets[g]], ig_out.at[:, sets[g]],
-                                          loc.at[5 + g, 0])]
-        return [
-            pltpu.make_async_copy(
-                mine.at[:, pl.ds(g * width + n * piece, piece)],
-                ig_out.at[:, pl.ds(n * m.df + g * piece, piece)], loc.at[5 + g, n])
-            for n in range(m.fs)
-        ]
+            ig_out[rows, sets[g]] = value
+            return
+        for n in range(m.fs):
+            ig_out[rows, pl.ds(n * m.df + g * piece, piece)] = value[:, n * piece:(n + 1) * piece]
+
+    def ig_final(first, g, terms):
+        def add(rows):
+            value = terms[0][rows, :].astype(F32)
+            for term in terms[1:]:
+                value = value + term[rows, :].astype(F32)
+            ig_store(pl.ds(aligned(first + rows.start, 32), rows.size), g, value)
+        by_rows(m.half, 32, add)
 
     def ig_last(g):
         ig_y1(g).wait_recv()
-        accumulate(crecv.at[y, x, low, sets[g]], [yr1.at[:, sets[g]]])
+        ig_final(0, g, [crecv.at[y, x, low, sets[g]], yr1.at[:, sets[g]]])
         for k in range(1, nx):
             ig_x2(g, k).wait_recv()
-        accumulate(crecv.at[y, x, high, sets[g]],
-                   [xr2.at[k, :, sets[g]] for k in range(nx - 1)])
-        for copy in ig_local(g):
-            copy.start()
+        ig_final(m.half, g, [crecv.at[y, x, high, sets[g]]]
+                 + [xr2.at[k, :, sets[g]] for k in range(nx - 1)])
 
     def acts_in(index):
         act_copy(index, True).wait_recv()
@@ -548,15 +555,15 @@
         for p in order[:2]:
             og_rows.start_y(p)
             og_rows.start_x(p)
-        go(act_copy(0))
+        act_copy(0).start()
         go(weight_y(DN))
         for p in order[2:]:
             og_rows.start_y(p)
-        go(act_copy(1))
+        act_copy(1).start()
         go(weight_y(UP))
-        go(act_copy(2))
+        act_copy(2).start()
         in_rows.start_y(0)
-        go(act_copy(3))
+        act_copy(3).start()
         ag_step(UP, 0, 0, 0)
         ag_step(UP, 0, 1, 0)
         for copy in local:
@@ -590,13 +597,13 @@
     def weight_in(w):
         weight_y(w, True).wait_recv()
 
+    def act_drain():
+        every = acts.at[pl.ds(0, m.rows), :]
+        remote(every, every, act_s, act_r.at[0], y_dev).wait_send()
+
     def ig_drain():
         for g in range(2):
-            @pl.loop(0, ny * nx)
-            def _(j):
-                ig_c(g, j).wait_send()
-            for copy in ig_local(g):
-                copy.wait()
+            ig_all(g).wait_send()
 
     def gather_on(w, u, h):
         near_steps = [(ag_step, w, u, h, k, "near") for k in range(2, nz // 2)]
@@ -707,6 +714,7 @@
         (rs_finish, UP, 3),
         (in_rows.drain,),
         (drain, sends),
+        (act_drain,),
         (ig_drain,),
         (rs_drain, DN),
         (rs_drain, UP),
@@ -725,18 +733,17 @@
     dma = pltpu.SemaphoreType.DMA
     vm = pltpu.VMEM
     any_space = pl.BlockSpec(memory_space=pl.ANY)
-    rows_events = 1 + 2 * (m.nx - 1) + m.ny * m.nx
     flops = 8 * m.all_rows * m.hh * m.d
     ig, ug, dg = pl.pallas_call(
         functools.partial(kernel, m),
         name="ffn_backward",
         out_shape=(
-            jax.ShapeDtypeStruct((m.t, m.d), BF16),
-            jax.ShapeDtypeStruct((m.df, m.h), BF16),
-            jax.ShapeDtypeStruct((m.h, m.df), BF16),
+            vm((m.t, m.d), BF16),
+            vm((m.df, m.h), BF16),
+            vm((m.h, m.df), BF16),
         ),
         in_specs=[any_space] * 5,
-        out_specs=(any_space,) * 3,
+        out_specs=(pl.BlockSpec(memory_space=pltpu.VMEM),) * 3,
         scratch_shapes=[
             vm((m.all_rows, m.d), BF16),
             vm((m.all_rows, m.d), BF16),
@@ -754,34 +761,79 @@
             vm((m.half, m.d), BF16),
             vm((m.nx, m.half, m.d), BF16),
             vm((m.nx - 1, m.half, m.d), BF16),
-            dma((7, m.fs)),
-            dma((2, m.ny, 2, 2, m.nz - 1)),
-            dma((2, m.ny, 2, 2, m.nz - 1)),
+            dma((5,)),
+            dma((3 * m.ny, 2, m.nz - 1)),
+            dma((3 * m.ny, m.nz)),
             dma((2,)),
             dma((2,)),
-            dma((2, rows_events * m.nz)),
-            dma((2, rows_events * m.nz)),
+            dma((2,)),
+            dma((m.nz + 1, 2 * m.nx)),
+            dma,
             dma((ACT_PARTS,)),
-            dma((ACT_PARTS,)),
-            dma((2, 2, m.nz, CHUNKS)),
-            dma((2, 2, m.nz, CHUNKS)),
-            dma((2, CHUNKS)),
-            dma((2, CHUNKS)),
-            dma((2, CHUNKS)),
-            dma((2, m.ny * m.nx)),
-            dma((2, m.ny * m.nx)),
-            dma((2, 4, m.nx)),
-            dma((2, 4, m.nx)),
+            dma((2, m.nz)),
+            dma((2, m.nz + 1, CHUNKS)),
+            dma((2,)),
+            dma((2,)),
+            dma((2,)),
+            dma((2,)),
+            dma((2, 2 * m.nx)),
+            dma((2, 2 * m.nx)),
         ],
         cost_estimate=pl.CostEstimate(flops=flops, bytes_accessed=2**25, transcendentals=0),
         compiler_params=pltpu.CompilerParams(
-            collective_id=0, has_side_effects=True, vmem_limit_bytes=67043328
+            collective_id=0, has_side_effects=True, vmem_limit_bytes=62914560
         ),
     )(inp, act, og, upw, dnw)
     if not m.direct:
         ig = ig.reshape(m.t, 2, m.fs, m.df // 2).transpose(0, 2, 1, 3)
         ig = ig.reshape(m.t, m.d)
-    return ig, ug.astype(F32), dg.astype(F32)
+    return widen(ig, ug, dg)
+
+
+def widen(ig, ug, dg):
+    steps = 2
+
+    def body(ig_in, ug_in, dg_in, ig_out, ug_out, dg_out, wide_ug, wide_dg, sems):
+        copies = [pltpu.make_async_copy(ig_in, ig_out, sems.at[0])]
+        copies[0].start()
+        pairs = ((ug_in, wide_ug, ug_out), (dg_in, wide_dg, dg_out))
+        for which, (src, wide, out) in enumerate(pairs):
+            count = src.shape[0] // steps
+            for i in range(steps):
+                first = i * count
+                rows = pl.ds(first, count)
+
+                @pl.loop(0, count // 32)
+                def _(j):
+                    part = pl.ds(aligned(first + j * 32, 32), 32)
+                    wide[part, :] = src[part, :].astype(F32)
+
+                copies.append(pltpu.make_async_copy(
+                    wide.at[rows, :], out.at[rows, :], sems.at[1 + which * steps + i]))
+                copies[-1].start()
+        for copy in copies:
+            copy.wait()
+
+    vmem = pl.BlockSpec(memory_space=pltpu.VMEM)
+    outside = pl.BlockSpec(memory_space=pl.ANY)
+    return pl.pallas_call(
+        body,
+        name="widen",
+        out_shape=(
+            jax.ShapeDtypeStruct(ig.shape, BF16),
+            jax.ShapeDtypeStruct(ug.shape, F32),
+            jax.ShapeDtypeStruct(dg.shape, F32),
+        ),
+        in_specs=[vmem] * 3,
+        out_specs=(outside,) * 3,
+        scratch_shapes=[
+            pltpu.VMEM(ug.shape, F32),
+            pltpu.VMEM(dg.shape, F32),
+            pltpu.SemaphoreType.DMA((1 + 2 * steps,)),
+        ],
+        cost_estimate=pl.CostEstimate(flops=ug.size, bytes_accessed=16 * ug.size, transcendentals=0),
+        compiler_params=pltpu.CompilerParams(vmem_limit_bytes=16 * ug.size),
+    )(*(pltpu.with_memory_space_constraint(v, pltpu.VMEM) for v in (ig, ug, dg)))
 
 
 def solution(mesh):

time: 202 us -> 196 us (0.970)
  other arithmetic: 4.36 us -> 0 us
    convert_element_type x2 -> x0, other arithmetic: 4.36 us -> none  [local_step(): return (ig, ug.astype(F32), dg.astype(F32))]
    pallas_call x1, Pallas kernels: 195 us -> 192 us  [local_step(): pl.pallas_call(functools.partial(kernel, m), name='ffn_backward', out_sha...]
    pallas_call x0 -> x1, Pallas kernels: none -> 2.31 us  [widen(): pl.pallas_call(body, name='widen', out_shape=(jax.ShapeDtypeStruct(ig.sha...]
where the time goes in v4:
time: 196 us; the launch traced here: 195 us
  Pallas kernels  194 us (99%)
    pallas_call x1, Pallas kernels, local_step(): pl.pallas_call(functools.partial(kernel, m), name='ffn_backward', out_sha...  192 us

profile of v4, /device:TPU:8, one launch (start us, length us, event | category | flops | bytes accessed | tf_op | source)
XLA Modules:
  0.0 194.6 jit_solution(4003681013712176595)
XLA Ops:
  0.6 191.7 %ffn_backward.1 = (bf16[192,2048]{1,0:T(8,128)(2,1)S(1)}, bf16[256,2048]{1,0:T(8,128)(2,1)S(1)}, bf16[2048,256]{1,0:T(8,128)(2,1)S(1)}) custom-call(bf16[192,2048]{1,0:T(8,128)(2,1)} %inp.1, bf16[768,2048]{1,0:T(8,128)(2,1)} %act.1, bf16[192,2048]{1,0:T(8,128)(2,1)} %og.1, bf16[256,2048]{1,0:T(8,128)(2,1)} %upw.1, bf16[2048,256]{1,0:T(8,128)(2,1)} %dnw.1), custom_call_target="tpu_custom_call" | custom-call | flops 25769803776 | bytes 33554432 | tf_op jit(solution)/shard_map/ffn_backward/pallas_call | solution.py:737
  192.3 2.3 %widen.1 = (bf16[192,2048]{1,0:T(8,128)(2,1)}, f32[256,2048]{1,0:T(8,128)}, f32[2048,256]{1,0:T(8,128)}) custom-call(bf16[192,2048]{1,0:T(8,128)(2,1)S(1)} %get-tuple-element.6.ig_in, bf16[256,2048]{1,0:T(8,128)(2,1)S(1)} %get-tuple-element.7.ug_in, bf16[2048,256]{1,0:T(8,128)(2,1)S(1)} %get-tuple-element.8.dg_in), custom_call_target="tpu_custom_call" | custom-call | flops 524288 | bytes 8388608 | tf_op jit(solution)/shard_map/widen/pallas_call | solution.py:819

commit v5 on v4

--- a/solution.py
+++ b/solution.py
@@ -41,7 +41,7 @@
     og_all, in_all, acts, hid, pre, dn_all, up_all,
     part_dn, part_up, slot_dn, slot_up, crecv, xr1, yr1, yr2, xr2,
     loc, ag_s, ag_r, wy_s, wy_r, tok_s, tok_r, act_s, act_r,
-    rs_s, rs_r, fin_s, fin_r, igc_s, igc_r, igx_s, igx_r,
+    rs_s, rs_r, rs_h, fin_s, fin_r, igc_s, igc_r, igx_s, igx_r,
 ):
     f, tt = lax.axis_index("fs"), lax.axis_index("tp")
     ny, nx, nz = m.ny, m.nx, m.nz
@@ -251,34 +251,43 @@
 
     parts, slots = (part_dn, part_up), (slot_dn, slot_up)
 
-    def rs(w, side, target, ch, own):
+    def half_of(ref, half):
+        if half is None:
+            return ref
+        yy = yo if half == 0 else y
+        return ref.at[pl.ds(aligned(yy * m.df, m.df), m.df), :]
+
+    def rs_sem(w, place, ch, half):
+        return rs_r.at[w, place, ch] if half != 1 else rs_h.at[place, ch]
+
+    def rs(w, side, target, ch, own, half=None):
         src = (parts if own else slots)[w].at[target, ch]
         if side == RIGHT:
             place = target
         else:
             place = jnp.where(target == z - 1, nz, target)
-        return remote(src, slots[w].at[place, ch], rs_s.at[w, target],
-                      rs_r.at[w, place, ch], z_dev[side])
-
-    def rs_waits(w, side, ch, place):
-        return remote(parts[w].at[0, ch], slots[w].at[place, ch], rs_s.at[w, 0],
-                      rs_r.at[w, place, ch], z_dev[side])
+        return remote(half_of(src, half), half_of(slots[w].at[place, ch], half),
+                      rs_s.at[w, target], rs_sem(w, place, ch, half), z_dev[side])
+
+    def rs_waits(w, side, ch, place, half=None):
+        return remote(half_of(parts[w].at[0, ch], half), half_of(slots[w].at[place, ch], half),
+                      rs_s.at[w, 0], rs_sem(w, place, ch, half), z_dev[side])
 
     def by_rows(count, step, body):
         @pl.loop(0, count // step)
         def _(i):
             body(pl.ds(aligned(i * step, step), step))
 
-    def rs_edge(w, target, ch):
+    def rs_edge(w, target, ch, half=None):
         @pl.when(jnp.logical_and(z == 0, target > 0))
         def _():
-            rs(w, RIGHT, target, ch, True).start()
+            rs(w, RIGHT, target, ch, True, half).start()
 
         @pl.when(jnp.logical_and(z == nz - 1, target < nz - 1))
         def _():
-            rs(w, LEFT, target, ch, True).start()
-
-    def rs_pass(w, side, step, ch):
+            rs(w, LEFT, target, ch, True, half).start()
+
+    def rs_pass(w, side, step, ch, half=None):
         target = nz - 1 - step if side == RIGHT else step
         if side == RIGHT:
             cond = jnp.logical_and(z > 0, z < target)
@@ -287,36 +296,37 @@
 
         @pl.when(cond)
         def _():
-            rs_waits(w, side, ch, target).wait_recv()
-            buf, own = slots[w].at[target, ch], parts[w].at[target, ch]
+            rs_waits(w, side, ch, target, half).wait_recv()
+            buf = half_of(slots[w].at[target, ch], half)
+            own = half_of(parts[w].at[target, ch], half)
 
             def add(rows):
                 buf[rows, :] = (buf[rows, :].astype(F32)
                                 + own[rows, :].astype(F32)).astype(BF16)
             by_rows(buf.shape[0], 64, add)
-            rs(w, side, target, ch, False).start()
+            rs(w, side, target, ch, False, half).start()
+
+    def passes(w, sides, chunks, first, last, half):
+        for low_side in (True, False):
+            @pl.when(z < nz // 2 if low_side else z >= nz // 2)
+            def _():
+                for step in range(first, last):
+                    for ch in chunks:
+                        rs_pass(w, sides[0] if low_side else sides[1], step, ch, half)
 
     def near(w, ch, first=0, last=nz - 2):
-        @pl.when(z < nz // 2)
-        def _():
-            for step in range(first, last):
-                rs_pass(w, RIGHT, step, ch)
-
-        @pl.when(z >= nz // 2)
-        def _():
-            for step in range(first, last):
-                rs_pass(w, LEFT, step, ch)
+        passes(w, (RIGHT, LEFT), [ch], first, last, None)
 
     def far(w, ch):
-        @pl.when(z < nz // 2)
-        def _():
-            for step in range(nz - 2):
-                rs_pass(w, LEFT, step, ch)
-
-        @pl.when(z >= nz // 2)
-        def _():
-            for step in range(nz - 2):
-                rs_pass(w, RIGHT, step, ch)
+        passes(w, (LEFT, RIGHT), [ch], 0, nz - 2, None)
+
+    tail = (CHUNKS - 2, CHUNKS - 1)
+
+    def near_tail(first, last, half):
+        passes(UP, (RIGHT, LEFT), tail, first, last, half)
+
+    def far_tail(half):
+        passes(UP, (LEFT, RIGHT), tail, 0, nz - 2, half)
 
     def rs_drain(w):
         for target in range(nz):
@@ -338,11 +348,11 @@
         return remote(fin_cut(w, parts[w].at[z, ch], yo), fin_place(w, ch, y),
                       fin_s.at[w], fin_r.at[w], y_dev)
 
-    def rs_finish(w, ch):
+    def rs_finish(w, ch, half=None):
         own = parts[w].at[z, ch]
         right, left = slots[w].at[z, ch], slots[w].at[nz, ch]
-        pl.when(z > 0)(rs_waits(w, RIGHT, ch, z).wait_recv)
-        pl.when(z < nz - 1)(rs_waits(w, LEFT, ch, nz).wait_recv)
+        pl.when(z > 0)(rs_waits(w, RIGHT, ch, z, half).wait_recv)
+        pl.when(z < nz - 1)(rs_waits(w, LEFT, ch, nz, half).wait_recv)
 
         def total(yy, dst, others):
             terms = [fin_cut(w, buf, yy) for buf in others]
@@ -360,9 +370,15 @@
             pl.when(jnp.logical_and(z > 0, z < nz - 1))(
                 lambda: total(yy, dst, (own, right, left)))
 
-        both(yo, fin_cut(w, own, yo))
-        fin_remote(w, ch).start()
-        both(y, fin_place(w, ch, y))
+        if half != 1:
+            both(yo, fin_cut(w, own, yo))
+            fin_remote(w, ch).start()
+        if half != 0:
+            both(y, fin_place(w, ch, y))
+
+    def finish_tail(half):
+        for ch in tail:
+            rs_finish(UP, ch, half)
 
     def fin_wait(w):
         def half(yy):
@@ -420,11 +436,12 @@
             if send:
                 rs_edge(UP, target, ch)
 
-    def up_sends(first):
-        @pl.loop(0, nz * (CHUNKS - first))
+    def up_sends():
+        @pl.loop(0, nz)
         def _(i):
-            count = CHUNKS - first
-            rs_edge(UP, targets(i // count), first + i % count)
+            for half in range(2):
+                for ch in tail:
+                    rs_edge(UP, targets(i), ch, half)
 
     part = og_all
     width = m.d // 2
@@ -679,7 +696,7 @@
         (ig_sum, 0),
         (ig_first, 0),
         (dot_up, 3, False),
-        (up_sends, 2),
+        (up_sends,),
         (far, DN, 0),
         (far, DN, 1),
         (near, UP, 0),
@@ -701,17 +718,17 @@
         (ig_second, 1),
         (rs_finish, DN, 2),
         (rs_finish, DN, 3),
-        (near, UP, 2, 0, 1),
+        (near_tail, 0, 1, 0),
         (ig_last, 1),
-        (near, UP, 3, 0, 1),
+        (near_tail, 0, 1, 1),
         (rs_finish, UP, 0),
-        (near, UP, 2, 1, nz - 2),
-        (far, UP, 2),
+        (near_tail, 1, nz - 2, 0),
+        (far_tail, 0),
         (rs_finish, UP, 1),
-        (near, UP, 3, 1, nz - 2),
-        (far, UP, 3),
-        (rs_finish, UP, 2),
-        (rs_finish, UP, 3),
+        (near_tail, 1, nz - 2, 1),
+        (far_tail, 1),
+        (finish_tail, 0),
+        (finish_tail, 1),
         (in_rows.drain,),
         (drain, sends),
         (act_drain,),
@@ -772,6 +789,7 @@
             dma((ACT_PARTS,)),
             dma((2, m.nz)),
             dma((2, m.nz + 1, CHUNKS)),
+            dma((m.nz + 1, CHUNKS)),
             dma((2,)),
             dma((2,)),
             dma((2,)),

time: 196 us -> 192 us (0.980)
  Pallas kernels: 194 us -> 190 us
    pallas_call x1, Pallas kernels: 192 us -> 187 us  [local_step(): pl.pallas_call(functools.partial(kernel, m), name='ffn_backward', out_sha...]
where the time goes in v5:
time: 192 us; the launch traced here: 190 us
  Pallas kernels  190 us (99%)
    pallas_call x1, Pallas kernels, local_step(): pl.pallas_call(functools.partial(kernel, m), name='ffn_backward', out_sha...  187 us

profile of v5, /device:TPU:8, one launch (start us, length us, event | category | flops | bytes accessed | tf_op | source)
XLA Modules:
  0.0 190.2 jit_solution(7216431877926669815)
XLA Ops:
  0.6 187.3 %ffn_backward.1 = (bf16[192,2048]{1,0:T(8,128)(2,1)S(1)}, bf16[256,2048]{1,0:T(8,128)(2,1)S(1)}, bf16[2048,256]{1,0:T(8,128)(2,1)S(1)}) custom-call(bf16[192,2048]{1,0:T(8,128)(2,1)} %inp.1, bf16[768,2048]{1,0:T(8,128)(2,1)} %act.1, bf16[192,2048]{1,0:T(8,128)(2,1)} %og.1, bf16[256,2048]{1,0:T(8,128)(2,1)} %upw.1, bf16[2048,256]{1,0:T(8,128)(2,1)} %dnw.1), custom_call_target="tpu_custom_call" | custom-call | flops 25769803776 | bytes 33554432 | tf_op jit(solution)/shard_map/ffn_backward/pallas_call | solution.py:754
  187.9 2.3 %widen.1 = (bf16[192,2048]{1,0:T(8,128)(2,1)}, f32[256,2048]{1,0:T(8,128)}, f32[2048,256]{1,0:T(8,128)}) custom-call(bf16[192,2048]{1,0:T(8,128)(2,1)S(1)} %get-tuple-element.6.ig_in, bf16[256,2048]{1,0:T(8,128)(2,1)S(1)} %get-tuple-element.7.ug_in, bf16[2048,256]{1,0:T(8,128)(2,1)S(1)} %get-tuple-element.8.dg_in), custom_call_target="tpu_custom_call" | custom-call | flops 524288 | bytes 8388608 | tf_op jit(solution)/shard_map/widen/pallas_call | solution.py:837

commit v6 on v5

--- a/solution.py
+++ b/solution.py
@@ -63,7 +63,7 @@
     def mirror(target):
         return jnp.where(z < nz // 2, target, nz - 1 - target)
 
-    order = [mirror(nz - 1 - i // 2 if i % 2 == 0 else i // 2) for i in range(nz)]
+    order = [mirror(nz - 1 - i) for i in range(nz)]
 
     def remote(src, dst, ss, rs, dev):
         return pltpu.make_async_remote_copy(
@@ -128,7 +128,7 @@
         view = weight_view(w, origin * ny + (y if u == 0 else yo), h)
         src = weight_own(w, y, h) if (u == 0 and k == 0) else view
         unit = u if w == DN else ny + 2 * u + h
-        return remote(src, view, ag_s.at[unit, side, k], ag_r.at[unit, origin], z_dev[side])
+        return remote(src, view, ag_s.at[side, k], ag_r.at[unit, origin], z_dev[side])
 
     def ag_sends(side, k):
         if side == RIGHT:
@@ -151,7 +151,14 @@
                 cond = jnp.logical_and(cond, close[1 - side])
             if k > 0:
                 pl.when(cond)(ag(w, u, h, side, k - 1, True).wait_recv)
-            go(ag(w, u, h, side, k), cond)
+            pl.when(cond)(ag(w, u, h, side, k).start)
+
+    def ag_drain():
+        every = up_all.at[pl.ds(0, 4 * m.df), :]
+        for side in (RIGHT, LEFT):
+            for k in range(nz - 1):
+                pl.when(ag_sends(side, k))(
+                    remote(every, every, ag_s.at[side, k], ag_r.at[0, 0], y_dev).wait_send)
 
     def ag_finish(w, u, h):
         for k in range(nz - 1):
@@ -258,7 +265,7 @@
         return ref.at[pl.ds(aligned(yy * m.df, m.df), m.df), :]
 
     def rs_sem(w, place, ch, half):
-        return rs_r.at[w, place, ch] if half != 1 else rs_h.at[place, ch]
+        return rs_r.at[w, place, ch] if half != 1 else rs_h.at[place, ch - tail[0]]
 
     def rs(w, side, target, ch, own, half=None):
         src = (parts if own else slots)[w].at[target, ch]
@@ -390,8 +397,7 @@
         remote(other, other, fin_s.at[w], fin_r.at[w], y_dev).wait_recv()
 
     def targets(i):
-        turn = i // 2
-        return mirror(jnp.where(i % 2 == 0, nz - 1 - turn, turn))
+        return mirror(nz - 1 - i)
 
     def squares(ch):
         cols = pl.ds(ch * m.hc, m.hc)
@@ -506,24 +512,24 @@
 
     def ig_x1(g, k):
         return remote(crecv.at[:, x_at(k), low, sets[g]], xr1.at[k - 1, :, :, sets[g]],
-                      igx_s.at[g, k - 1], igx_r.at[g, k - 1], at(z, y, x_at(k), c))
+                      igx_s.at[g], igx_r.at[g, k - 1], at(z, y, x_at(k), c))
 
     def ig_y1(g):
         return remote(crecv.at[yo, x, low, sets[g]], yr1.at[:, sets[g]],
-                      igx_s.at[g, nx - 1], igx_r.at[g, nx - 1], y_dev)
+                      igx_s.at[g], igx_r.at[g, nx - 1], y_dev)
 
     def ig_y2(g):
         return remote(crecv.at[yo, :, high, sets[g]], yr2.at[:, :, sets[g]],
-                      igx_s.at[g, nx], igx_r.at[g, nx], y_dev)
+                      igx_s.at[g], igx_r.at[g, nx], y_dev)
 
     def ig_x2(g, k):
         return remote(crecv.at[y, x_at(k), high, sets[g]], xr2.at[k - 1, :, sets[g]],
-                      igx_s.at[g, nx + k], igx_r.at[g, nx + k], at(z, y, x_at(k), c))
+                      igx_s.at[g], igx_r.at[g, nx + k], at(z, y, x_at(k), c))
 
     def ig_first(g):
         for k in range(1, nx):
-            go(ig_x1(g, k))
-        go(ig_y2(g))
+            ig_x1(g, k).start()
+        ig_y2(g).start()
 
     def ig_second(g):
         for k in range(1, nx):
@@ -531,12 +537,12 @@
         for yy in range(ny):
             accumulate(crecv.at[yy, x, low, sets[g]],
                        [xr1.at[k, yy, :, sets[g]] for k in range(nx - 1)])
-        go(ig_y1(g))
+        ig_y1(g).start()
         ig_y2(g).wait_recv()
         for xx in range(nx):
             accumulate(crecv.at[y, xx, high, sets[g]], [yr2.at[xx, :, sets[g]]])
         for k in range(1, nx):
-            go(ig_x2(g, k))
+            ig_x2(g, k).start()
 
     piece = m.df // 2
 
@@ -569,43 +575,33 @@
 
     def start():
         ag_step(DN, 0, 0, 0)
+        ag_step(UP, 0, 0, 0)
+        ag_step(UP, 0, 1, 0)
         for p in order[:2]:
+            og_rows.start_x(p)
+        og_rows.start_y(order[0])
+        act_copy(0).start()
+        for p in order[1:-1]:
             og_rows.start_y(p)
-            og_rows.start_x(p)
-        act_copy(0).start()
         go(weight_y(DN))
-        for p in order[2:]:
-            og_rows.start_y(p)
         act_copy(1).start()
+        og_rows.start_y(order[-1])
         go(weight_y(UP))
         act_copy(2).start()
         in_rows.start_y(0)
         act_copy(3).start()
-        ag_step(UP, 0, 0, 0)
-        ag_step(UP, 0, 1, 0)
         for copy in local:
             copy.start()
 
-    def first_rows():
-        for p in order[:2]:
-            og_rows.relay_y(p)
-            og_rows.relay_x(p, 0)
-        for p in order[2:]:
-            og_rows.start_x(p)
-
-    def first_rows_in():
-        for p in order[:2]:
-            og_rows.relay_x(p, 1)
-        for p in order[:2]:
-            og_rows.finish(p)
-
-    def more_rows(p):
-        og_rows.relay_y(p)
-        og_rows.relay_x(p, 0)
-
-    def more_rows_in(p):
-        og_rows.relay_x(p, 1)
-        og_rows.finish(p)
+    def rows_on(i):
+        og_rows.relay_y(order[i])
+        og_rows.relay_x(order[i], 0)
+        if i + 2 < nz:
+            og_rows.start_x(order[i + 2])
+
+    def rows_in(i):
+        og_rows.relay_x(order[i], 1)
+        og_rows.finish(order[i])
 
     def local_wait():
         for copy in local:
@@ -614,6 +610,14 @@
     def weight_in(w):
         weight_y(w, True).wait_recv()
 
+    def in_relay(edge):
+        outer = jnp.logical_or(z == 0, z == nz - 1)
+
+        @pl.when(outer if edge else jnp.logical_not(outer))
+        def _():
+            in_rows.relay_y(0)
+            in_rows.relay_x(0, 0)
+
     def act_drain():
         every = acts.at[pl.ds(0, m.rows), :]
         remote(every, every, act_s, act_r.at[0], y_dev).wait_send()
@@ -621,6 +625,8 @@
     def ig_drain():
         for g in range(2):
             ig_all(g).wait_send()
+            every = part.at[pl.ds(0, (2 * nx - 1) * m.t), sets[g]]
+            remote(every, every, igx_s.at[g], igx_r.at[g, 0], y_dev).wait_send()
 
     def gather_on(w, u, h):
         near_steps = [(ag_step, w, u, h, k, "near") for k in range(2, nz // 2)]
@@ -628,38 +634,43 @@
 
     plan = [
         (start,),
-        (first_rows,),
+        (rows_on, 0),
         (ag_step, DN, 0, 0, 1),
-        (first_rows_in,),
+        (rows_in, 0),
         (local_wait,),
         (acts_in, 0),
         (squares, 0),
-        (dot_dn, 0, 0, 2),
-        *gather_on(DN, 0, 0),
+        (dot_dn, 0, 0, 1),
+        *[(rows_on, i) for i in range(1, nz - 1)],
+        *[call for i in range(1, nz - 1)
+          for call in ((rows_in, i), (dot_dn, 0, i, i + 1))],
+        (near, DN, 0, 0, 1),
         (weight_in, DN),
         (ag_step, DN, 1, 0, 0),
-        (near, DN, 0, 0, 1),
-        *[(more_rows, p) for p in order[2:]],
-        (in_rows.start_x, 0),
-        *[call for i, p in enumerate(order[2:])
-          for call in ((more_rows_in, p), (dot_dn, 0, i + 2, i + 3))],
-        (ag_step, DN, 1, 0, 1),
+        *gather_on(DN, 0, 0),
+        (near, DN, 0, 1, nz - 2),
         (acts_in, 1),
         (squares, 1),
-        (dot_dn, 1),
-        (near, DN, 0, 1, nz - 2),
-        *gather_on(DN, 1, 0),
+        (dot_dn, 1, 0, nz - 1),
+        (rows_on, nz - 1),
+        (in_rows.start_x, 0),
+        (ag_step, DN, 1, 0, 1),
+        (rows_in, nz - 1),
+        (dot_dn, 0, nz - 1, nz),
+        (dot_dn, 1, nz - 1, nz),
         (weight_in, UP),
         (ag_step, UP, 1, 0, 0, "edge"),
         (ag_step, UP, 1, 1, 0, "edge"),
         (ag_step, UP, 1, 0, 0, "inner"),
         (ag_step, UP, 0, 0, 1, "near"),
+        (near, DN, 1),
         (acts_in, 2),
         (squares, 2),
         (dot_dn, 2),
-        (near, DN, 1),
+        *gather_on(DN, 1, 0),
         (ag_step, UP, 0, 0, 1, "far"),
         (ag_step, UP, 1, 0, 1, "near"),
+        (in_relay, True),
         (ag_finish, DN, 0, 0),
         (ag_finish, DN, 1, 0),
         (dot_hg, 0),
@@ -669,8 +680,7 @@
         (ag_step, UP, 1, 1, 0, "inner"),
         (ag_step, UP, 0, 1, 1, "near"),
         (ag_step, UP, 1, 1, 1, "near"),
-        (in_rows.relay_y, 0),
-        (in_rows.relay_x, 0, 0),
+        (in_relay, False),
         *gather_on(UP, 0, 0),
         *gather_on(UP, 1, 0),
         (acts_in, 3),
@@ -731,6 +741,7 @@
         (finish_tail, 1),
         (in_rows.drain,),
         (drain, sends),
+        (ag_drain,),
         (act_drain,),
         (ig_drain,),
         (rs_drain, DN),
@@ -779,7 +790,7 @@
             vm((m.nx, m.half, m.d), BF16),
             vm((m.nx - 1, m.half, m.d), BF16),
             dma((5,)),
-            dma((3 * m.ny, 2, m.nz - 1)),
+            dma((2, m.nz - 1)),
             dma((3 * m.ny, m.nz)),
             dma((2,)),
             dma((2,)),
@@ -789,12 +800,12 @@
             dma((ACT_PARTS,)),
             dma((2, m.nz)),
             dma((2, m.nz + 1, CHUNKS)),
-            dma((m.nz + 1, CHUNKS)),
+            dma((m.nz + 1, 2)),
             dma((2,)),
             dma((2,)),
             dma((2,)),
             dma((2,)),
-            dma((2, 2 * m.nx)),
+            dma((2,)),
             dma((2, 2 * m.nx)),
         ],
         cost_estimate=pl.CostEstimate(flops=flops, bytes_accessed=2**25, transcendentals=0),

time: 192 us -> 191 us (level)
  Pallas kernels: 190 us -> 188 us
where the time goes in v6:
time: 191 us; the launch traced here: 188 us
  Pallas kernels  188 us (98%)
    pallas_call x1, Pallas kernels, local_step(): pl.pallas_call(functools.partial(kernel, m), name='ffn_backward', out_sha...  185 us

profile of v6, /device:TPU:8, one launch (start us, length us, event | category | flops | bytes accessed | tf_op | source)
XLA Modules:
  0.0 188.3 jit_solution(14247960157947974602)
XLA Ops:
  0.6 185.4 %ffn_backward.1 = (bf16[192,2048]{1,0:T(8,128)(2,1)S(1)}, bf16[256,2048]{1,0:T(8,128)(2,1)S(1)}, bf16[2048,256]{1,0:T(8,128)(2,1)S(1)}) custom-call(bf16[192,2048]{1,0:T(8,128)(2,1)} %inp.1, bf16[768,2048]{1,0:T(8,128)(2,1)} %act.1, bf16[192,2048]{1,0:T(8,128)(2,1)} %og.1, bf16[256,2048]{1,0:T(8,128)(2,1)} %upw.1, bf16[2048,256]{1,0:T(8,128)(2,1)} %dnw.1), custom_call_target="tpu_custom_call" | custom-call | flops 25769803776 | bytes 33554432 | tf_op jit(solution)/shard_map/ffn_backward/pallas_call | solution.py:765
  186.0 2.3 %widen.1 = (bf16[192,2048]{1,0:T(8,128)(2,1)}, f32[256,2048]{1,0:T(8,128)}, f32[2048,256]{1,0:T(8,128)}) custom-call(bf16[192,2048]{1,0:T(8,128)(2,1)S(1)} %get-tuple-element.6.ig_in, bf16[256,2048]{1,0:T(8,128)(2,1)S(1)} %get-tuple-element.7.ug_in, bf16[2048,256]{1,0:T(8,128)(2,1)S(1)} %get-tuple-element.8.dg_in), custom_call_target="tpu_custom_call" | custom-call | flops 524288 | bytes 8388608 | tf_op jit(solution)/shard_map/widen/pallas_call | solution.py:848

commit v7 on v6

--- a/solution.py
+++ b/solution.py
@@ -820,7 +820,7 @@
 
 
 def widen(ig, ug, dg):
-    steps = 2
+    steps = 4
 
     def body(ig_in, ug_in, dg_in, ig_out, ug_out, dg_out, wide_ug, wide_dg, sems):
         copies = [pltpu.make_async_copy(ig_in, ig_out, sems.at[0])]

time: 191 us -> 191 us (level)
  no operation moved by 1% of the time
where the time goes in v7:
time: 191 us; the launch traced here: 188 us
  Pallas kernels  188 us (98%)
    pallas_call x1, Pallas kernels, local_step(): pl.pallas_call(functools.partial(kernel, m), name='ffn_backward', out_sha...  185 us

profile of v7, /device:TPU:8, one launch (start us, length us, event | category | flops | bytes accessed | tf_op | source)
XLA Modules:
  0.0 188.3 jit_solution(10083457077075780842)
XLA Ops:
  0.6 185.4 %ffn_backward.1 = (bf16[192,2048]{1,0:T(8,128)(2,1)S(1)}, bf16[256,2048]{1,0:T(8,128)(2,1)S(1)}, bf16[2048,256]{1,0:T(8,128)(2,1)S(1)}) custom-call(bf16[192,2048]{1,0:T(8,128)(2,1)} %inp.1, bf16[768,2048]{1,0:T(8,128)(2,1)} %act.1, bf16[192,2048]{1,0:T(8,128)(2,1)} %og.1, bf16[256,2048]{1,0:T(8,128)(2,1)} %upw.1, bf16[2048,256]{1,0:T(8,128)(2,1)} %dnw.1), custom_call_target="tpu_custom_call" | custom-call | flops 25769803776 | bytes 33554432 | tf_op jit(solution)/shard_map/ffn_backward/pallas_call | solution.py:765
  186.0 2.3 %widen.1 = (bf16[192,2048]{1,0:T(8,128)(2,1)}, f32[256,2048]{1,0:T(8,128)}, f32[2048,256]{1,0:T(8,128)}) custom-call(bf16[192,2048]{1,0:T(8,128)(2,1)S(1)} %get-tuple-element.6.ig_in, bf16[256,2048]{1,0:T(8,128)(2,1)S(1)} %get-tuple-element.7.ug_in, bf16[2048,256]{1,0:T(8,128)(2,1)S(1)} %get-tuple-element.8.dg_in), custom_call_target="tpu_custom_call" | custom-call | flops 524288 | bytes 8388608 | tf_op jit(solution)/shard_map/widen/pallas_call | solution.py:848
